TPU v7x, 32 devices: a whole 2x2x4 slice. The times are simulated.
32 devices in a mesh: ep: 8 (over z, core), tp: 4 (over y, x).
Axes of the slice: x: 2, y: 2, z: 4, core: 2. Of those that a mesh axis runs over, the one named last changes fastest.
Arguments:
- stream: bfloat16 [128, 4096], P('ep'), may hold values from -6 to 6
- previous_state: float32 [128, 128, 4096], P('ep', None, 'tp'), may hold values from -6 to 6
- mixer_norm_gain: float32 [4096], replicated, may hold values from 0.1 to 1.9
- query_matrix: bfloat16 [4096, 2048], P('ep'), may hold values from -0.09375 to 0.09375
- key_matrix: bfloat16 [4096, 2048], P('ep'), may hold values from -0.09375 to 0.09375
- value_matrix: bfloat16 [4096, 4096], P('ep', 'tp'), may hold values from -0.09375 to 0.09375
- output_gate_weight: bfloat16 [4096, 4096], P('ep', 'tp'), may hold values from -0.09375 to 0.09375
- decay_lower_factor: bfloat16 [4096, 64], replicated, may hold values from -0.09375 to 0.09375
- decay_upper_factor: bfloat16 [64, 2048], replicated, may hold values from -3 to 3
- forgetting_boost: float32 [128, 2048], P('ep'), may hold values from 0.02 to 1.5
- head_norm_gain: float32 [256], replicated, may hold values from 0.1 to 1.9
- output_matrix: bfloat16 [4096, 4096], P('tp'), may hold values from -0.1875 to 0.1875
- mixture_norm_gain: float32 [4096], replicated, may hold values from 0.1 to 1.9
- expert_gate_weight: bfloat16 [8, 1024, 4096], P('ep', 'tp'), may hold values from -0.09375 to 0.09375
- expert_up_weight: bfloat16 [8, 1024, 4096], P('ep', 'tp'), may hold values from -0.09375 to 0.09375
- expert_down_weight: bfloat16 [8, 1024, 4096], P('ep', None, 'tp'), may hold values from -0.375 to 0.375
- expert_index_table: int32 [128, 2], P('ep'), may hold values from 0 to 7, as said below
- expert_scores_within: float32 [128, 2], P('ep'), may hold values from -6 to 6
- group_probability: float32 [128], P('ep'), may hold values from 0.3 to 1
Outputs:
- new_stream: bfloat16 [128, 4096], P('ep', 'tp')
- new_state: float32 [128, 128, 4096], P('ep', None, 'tp')
Inputs may be any that keep to these rules, and one draw needn't show every extreme that they name: `expert_index_table`: the 2 experts of a sequence are distinct and lie in one group of 2 consecutive experts. Among the 16 sequences of one index of ep (aligned blocks of rows), each expert is named at most 8 times, and in every block some experts are named exactly 8 times.
All inputs are finite; a program needn't handle non-finite values.
Results may differ from a plain program's by a relative error of at most 0.02.
Values may be sent and summed in bfloat16 or wider, within the bound.
A program may use at most 128 MiB of HBM per device.

v0:
```python
import jax
import jax.numpy as jnp
from jax import lax
from jax.sharding import PartitionSpec as P

HEAD_TOTAL = 16
KEY_CHANNELS = 128
DV = 256


epsilon = 1e-06
forgetting_softness = 16.0


def rms_scaled(values, gain_vec):
    floats = values.astype(jnp.float32)
    scaled = floats * lax.rsqrt(jnp.mean(floats * floats, axis=-1, keepdims=True) + epsilon)
    return (scaled * gain_vec).astype(jnp.bfloat16)


def on_device(
    stream,
    previous_state,
    mixer_norm_gain,
    query_matrix,
    key_matrix,
    value_matrix,
    output_gate_weight,
    decay_lower_factor,
    decay_upper_factor,
    forgetting_boost,
    head_norm_gain,
    output_matrix,
    mixture_norm_gain,
    expert_gate_weight,
    expert_up_weight,
    expert_down_weight,
    expert_index_table,
    expert_scores_within,
    group_probability,
):
    seq_count, model_width = stream.shape
    value_local = previous_state.shape[2]
    head_count = max(1, value_local // DV)
    head_width = min(value_local, DV)
    tp_index = lax.axis_index("tp")
    leading_head = tp_index * value_local // DV
    value_start = tp_index * value_local % DV
    key_column_span = head_count * KEY_CHANNELS
    normed = rms_scaled(stream, mixer_norm_gain)
    own_query = lax.dynamic_slice_in_dim(
        query_matrix, leading_head * KEY_CHANNELS, key_column_span, 1
    )
    own_key = lax.dynamic_slice_in_dim(key_matrix, leading_head * KEY_CHANNELS, key_column_span, 1)
    spread = lax.all_to_all(normed, "ep", split_axis=1, concat_axis=0, tiled=True)
    joined = jnp.concatenate([own_query, own_key, value_matrix, output_gate_weight], axis=1)
    summed = lax.psum_scatter(
        jnp.dot(spread, joined, preferred_element_type=jnp.float32),
        "ep",
        scatter_dimension=0,
        tiled=True,
    )
    query_sum = summed[:, :key_column_span]
    key_sum = summed[:, key_column_span : 2 * key_column_span]
    value_sum = summed[:, 2 * key_column_span : 2 * key_column_span + value_local]
    gate_sum = summed[:, 2 * key_column_span + value_local :]
    queries = (query_sum * KEY_CHANNELS ** (-0.5)).astype(jnp.bfloat16)
    key_rows = key_sum.astype(jnp.bfloat16)
    value_rows = value_sum.astype(jnp.bfloat16)
    gate_rows = gate_sum.astype(jnp.bfloat16)
    low_rank = jnp.dot(normed, decay_lower_factor, preferred_element_type=jnp.float32).astype(
        jnp.bfloat16
    )
    local_expand_matrix = lax.dynamic_slice_in_dim(
        decay_upper_factor, leading_head * KEY_CHANNELS, key_column_span, 1
    )
    forgetting_logit = jnp.dot(low_rank, local_expand_matrix, preferred_element_type=jnp.float32)
    request_boost = lax.dynamic_slice_in_dim(
        forgetting_boost, leading_head * KEY_CHANNELS, key_column_span, 1
    )
    forgetting_lograte = jax.nn.log_sigmoid(forgetting_logit) / forgetting_softness - request_boost
    factor = (
        jnp.exp(forgetting_lograte)
        .reshape(seq_count, head_count, KEY_CHANNELS)
        .transpose(0, 2, 1)[..., None]
    )
    state_four = previous_state.reshape(seq_count, KEY_CHANNELS, head_count, head_width)
    key_part = (
        key_rows.astype(jnp.float32)
        .reshape(seq_count, head_count, KEY_CHANNELS)
        .transpose(0, 2, 1)[..., None]
    )
    value_part = value_rows.astype(jnp.float32).reshape(seq_count, 1, head_count, head_width)
    updated = factor * state_four + key_part * value_part
    query_part = (
        queries.astype(jnp.float32).reshape(seq_count, head_count, KEY_CHANNELS).transpose(0, 2, 1)
    )
    readout = jnp.einsum("skh,skhv->shv", query_part, updated, precision=lax.Precision.HIGHEST)
    square_sums = jnp.sum(readout * readout, axis=-1)
    norm_table = lax.dynamic_update_slice(
        jnp.zeros((seq_count, HEAD_TOTAL), jnp.float32), square_sums, (jnp.int32(0), leading_head)
    )
    totals = lax.psum(norm_table, "tp")
    own_totals = lax.dynamic_slice_in_dim(totals, leading_head, head_count, 1)
    mean_sq = own_totals[..., None] / DV
    own_gain = lax.dynamic_slice_in_dim(head_norm_gain, value_start, head_width, 0)
    gate_part = jax.nn.silu(
        gate_rows.astype(jnp.float32).reshape(seq_count, head_count, head_width)
    )
    gated_rows = (
        (readout * lax.rsqrt(mean_sq + epsilon) * own_gain * gate_part)
        .reshape(seq_count, value_local)
        .astype(jnp.bfloat16)
    )
    partial_out = jnp.dot(gated_rows, output_matrix, preferred_element_type=jnp.float32)
    mixer_sum = lax.psum(partial_out.astype(jnp.bfloat16), "tp").astype(jnp.float32)
    blended_tokens = (stream.astype(jnp.float32) + mixer_sum).astype(jnp.bfloat16)
    normed_two = rms_scaled(blended_tokens, mixture_norm_gain)
    ep_count = lax.axis_size("ep")
    local_experts = expert_gate_weight.shape[0]
    experts_all = ep_count * local_experts
    route_count = expert_index_table.shape[1]
    capacity = 2 * seq_count * route_count // experts_all
    slot_count = experts_all * capacity
    flat_ids = expert_index_table.reshape(seq_count * route_count)
    one_hot = (flat_ids[:, None] == jnp.arange(experts_all, dtype=jnp.int32)[None, :]).astype(
        jnp.int32
    )
    rank_in = jnp.sum(one_hot * (jnp.cumsum(one_hot, axis=0) - 1), axis=1)
    place_lookup = flat_ids * capacity + rank_in
    placing = (place_lookup[:, None] == jnp.arange(slot_count, dtype=jnp.int32)[None, :]).astype(
        jnp.float32
    )
    placing = placing.reshape(seq_count, route_count, slot_count)
    logit_exp = jnp.exp(expert_scores_within)
    weights = logit_exp / jnp.sum(logit_exp, axis=-1, keepdims=True) * group_probability[:, None]
    combine = jnp.einsum("sk,skc->sc", weights, placing, precision=lax.Precision.HIGHEST)
    dispatch = jnp.sum(placing, axis=1).astype(jnp.bfloat16)
    outgoing = jnp.einsum("sc,sd->cd", dispatch, normed_two, preferred_element_type=jnp.float32)
    outgoing = outgoing.astype(jnp.bfloat16).reshape(experts_all, capacity, model_width)
    width_local = expert_down_weight.shape[2]
    arrived = lax.all_to_all(outgoing, "ep", split_axis=0, concat_axis=0, tiled=True)
    held_slots = arrived.shape[1]
    grouped = arrived.reshape(ep_count, local_experts, held_slots, model_width)
    gate_pre = jnp.einsum(
        "sxcd,xfd->sxcf", grouped, expert_gate_weight, preferred_element_type=jnp.float32
    )
    up_pre = jnp.einsum(
        "sxcd,xfd->sxcf", grouped, expert_up_weight, preferred_element_type=jnp.float32
    )
    hidden = (jax.nn.silu(gate_pre) * up_pre).astype(jnp.bfloat16)
    outputs = jnp.einsum(
        "sxcf,xfd->sxcd",
        lax.all_gather(hidden, "tp", axis=3, tiled=True),
        expert_down_weight,
        preferred_element_type=jnp.float32,
    )
    ready_rows = outputs.astype(jnp.bfloat16).reshape(
        ep_count * local_experts, held_slots, width_local
    )
    returned = lax.all_to_all(ready_rows, "ep", split_axis=0, concat_axis=0, tiled=True)
    mixture = jnp.dot(
        combine,
        returned.reshape(slot_count, width_local).astype(jnp.float32),
        precision=lax.Precision.HIGHEST,
    )
    own_mixed = lax.dynamic_slice_in_dim(blended_tokens, tp_index * width_local, width_local, 1)
    new_stream = (own_mixed.astype(jnp.float32) + mixture).astype(jnp.bfloat16)
    return (new_stream, updated.reshape(seq_count, KEY_CHANNELS, value_local))


def solution(mesh):
    placed = (
        P("ep", None),
        P("ep", None, "tp"),
        P(),
        P("ep", None),
        P("ep", None),
        P("ep", "tp"),
        P("ep", "tp"),
        P(),
        P(),
        P("ep", None),
        P(),
        P("tp", None),
        P(),
        P("ep", "tp", None),
        P("ep", "tp", None),
        P("ep", None, "tp"),
        P("ep", None),
        P("ep", None),
        P("ep"),
    )
    return jax.shard_map(
        on_device,
        mesh=mesh,
        in_specs=placed,
        out_specs=(P("ep", "tp"), P("ep", None, "tp")),
        check_vma=False,
    )
```

profile of v0, /device:TPU:0, one launch (start us, length us, event | category | flops | bytes accessed | tf_op | source)
XLA Modules:
  0.0 207.3 jit_solution(5548687518825373681)
XLA Ops:
  7.2 0.0 copy-start
  7.2 1.2 fusion.36
  8.4 1.0 fusion.38
  9.4 0.7 copy.61
  10.1 6.4 %all-to-all-start = ((bf16[16,8,512]{2,0,1:T(8,128)(2,1)}), bf16[16,8,512]{2,0,1:T(8,128)(2,1)S(1)}, u32[]{:S(2)}, u32[]{:S(2)}) async-start(bf16[16,8,512]{2,0,1:T(8,128)(2,1)} %bitcast.84), calls=%async_computation | async-start | bytes 262144 | tf_op jit(solution)/shard_map/all_to_all | solution.py:55
  16.4 0.0 reduce-scatter.2.cloned.1.call-start
  16.5 1.3 constant_dynamic-slice_fusion
  17.8 5.4 %all-to-all-done = bf16[16,8,512]{2,0,1:T(8,128)(2,1)S(1)} async-done(((bf16[16,8,512]{2,0,1:T(8,128)(2,1)}), bf16[16,8,512]{2,0,1:T(8,128)(2,1)S(1)}, u32[]{:S(2)}, u32[]{:S(2)}) %all-to-all-start) | async-done | bytes 131104 | tf_op jit(solution)/shard_map/all_to_all | solution.py:55
  23.2 3.3 %fusion.3 = f32[128,3072]{1,0:T(8,128)} fusion(bf16[128,512]{1,0:T(8,128)(2,1)S(1)} %bitcast.90, bf16[512,1024]{1,0:T(8,128)(2,1)} %param.25, bf16[512,1024]{1,0:T(8,128)(2,1)} %param.24, bf16[512,512]{1,0:T(8,128)(2,1)S(1)} %get-tuple-element.6, bf16[512,512]{1,0:T(8,128)(2,1)S(1)} %get-tuple-element.7), kind=kOutput, calls=%fused_computation.7 | convolution fusion | flops 415236096 | bytes 4849664 | tf_op jit(solution)/shard_map/dot_general | solution.py:58
  26.5 0.0 reduce-scatter.2.cloned.1.call-update
  26.5 0.0 all-reduce.2.cloned.1.call-start
  26.5 0.0 copy-done.5
  26.6 0.1 copy.42
  26.6 0.1 eq.32
  26.7 0.1 fusion.60
  26.8 0.1 reduce_window_sum.11
  26.9 0.2 select_reduce_fusion
  27.0 0.1 reduce_sum.60
  27.1 0.1 copy.43
  27.2 10.6 %reshape.119 = f32[16,128,4,256]{3,2,1,0:T(4,128)} reshape(f32[16,128,1024]{2,1,0:T(8,128)} %param.20) | data formatting | bytes 16777216 | tf_op jit(solution)/shard_map/reshape | solution.py:87
  37.8 0.0 copy-done.3
  37.8 1.3 fusion.53
  39.1 0.4 copy.40
  39.5 20.4 %reduce-scatter.2.cloned.1.call-done = f32[16,3072]{1,0:T(8,128)} async-done(((f32[128,3072]{1,0:T(8,128)}), f32[16,3072]{1,0:T(8,128)}) %reduce-scatter.2.cloned.1.call-update) | async-done | bytes 196624 | tf_op jit(solution)/shard_map/reduce_scatter | solution.py:57
  59.9 0.9 convert.8
  61.0 1.4 copy.41
  62.4 0.8 fusion.54
  63.2 6.4 %multiply_add_fusion.1 = f32[16,128,4,256]{3,2,1,0:T(4,128)S(1)} fusion(f32[16,128,4,256]{3,2,1,0:T(4,128)} %reshape.119, f32[16,4,256]{2,1,0:T(4,128)S(1)} %mul.156, f32[16,128,4]{2,1,0:T(8,128)} %copy.41, f32[16,128,4]{2,1,0:T(8,128)S(1)} %copy.40), kind=kLoop, calls=%fused_computation.3 | loop fusion | flops 6291456 | bytes 16908288 | tf_op jit(solution)/shard_map/add | solution.py:94
  69.6 0.0 copy-start.6
  69.6 3.4 %fusion = f32[16,4,1,256]{3,2,1,0:T(1,128)S(1)} fusion(f32[16,128,4,256]{3,2,1,0:T(4,128)S(1)} %multiply_add_fusion.1, bf16[16,128,4,1]{1,2,0,3:T(4,128)(2,1)S(1)} %bitcast.87), kind=kOutput, calls=%fused_computation | convolution fusion | flops 25165824 | bytes 8470528 | tf_op jit(solution)/shard_map/skh,skhv->shv/dot_general | solution.py:98
  73.0 0.1 fusion.46
  73.1 0.2 dynamic_update_slice.3
  73.4 10.2 %psum.14 = f32[16,16]{1,0:T(8,128)S(1)} all-reduce(f32[16,16]{1,0:T(8,128)S(1)} %dynamic_update_slice.3), channel_id=1, replica_groups=mesh['ep'=8,'tp'=4] {'tp'}, use_global_device_ids=true, to_apply=%region_3.4 | all-reduce | flops 256 | bytes 2048 | tf_op jit(solution)/shard_map/psum | solution.py:103
  83.6 0.1 add_rsqrt_fusion
  83.7 0.0 copy-done.6
  83.7 0.1 fusion.49
  83.8 0.0 copy-start.2
  83.8 0.0 copy-start.4
  83.8 0.0 copy-start.7
  83.8 0.0 copy-start.8
  83.9 5.3 %convolution_convert_fusion.1 = bf16[16,4096]{1,0:T(8,128)(2,1)} fusion(bf16[16,1024]{1,0:T(8,128)(2,1)S(1)} %bitcast.86, bf16[1024,4096]{1,0:T(8,128)(2,1)} %param.30), kind=kOutput, calls=%fused_computation.6 | convolution fusion | flops 134283264 | bytes 8552448 | tf_op jit(solution)/shard_map/dot_general | solution.py:115
  89.2 0.0 all-reduce.2.cloned.1.call-update
  89.2 0.1 convert_reduce_fusion
  89.3 38.6 %all-reduce.2.cloned.1.call-done = bf16[16,4096]{1,0:T(8,128)(2,1)} async-done(((bf16[16,4096]{1,0:T(8,128)(2,1)}), bf16[16,4096]{1,0:T(8,128)(2,1)}) %all-reduce.2.cloned.1.call-update) | async-done | bytes 131088 | tf_op jit(solution)/shard_map/psum | solution.py:116
  127.9 1.1 fusion.33
  128.9 0.0 copy-done.4
  129.0 1.2 fusion.2
  130.1 4.6 %all-to-all-start.1 = ((bf16[8,8,4096]{2,1,0:T(8,128)(2,1)}), bf16[8,8,4096]{2,1,0:T(8,128)(2,1)}, u32[]{:S(2)}, u32[]{:S(2)}) async-start(bf16[8,8,4096]{2,1,0:T(8,128)(2,1)} %fusion.2), calls=%async_computation.2 | async-start | bytes 1048576 | tf_op jit(solution)/shard_map/all_to_all | solution.py:142
  134.8 0.1 copy.47
  134.8 4.5 %mul.153 = f32[16,128,4,256]{3,2,1,0:T(4,128)} broadcast(f32[16,128,4]{2,1,0:T(8,128)S(1)} %copy.40), dimensions={0,1,2} | broadcast | bytes 8421376 | tf_op jit(solution)/shard_map/mul | solution.py:94
  139.4 10.8 %mul.178 = f32[16,128,1024]{2,1,0:T(8,128)} reshape(f32[16,128,4,256]{3,2,1,0:T(4,128)} %mul.153) | data formatting | bytes 16777216 | tf_op jit(solution)/shard_map/mul | solution.py:94
  150.2 0.1 iota_compare_fusion
  150.3 0.2 fusion.58
  150.5 4.6 %mul.155 = f32[16,128,4,256]{3,2,1,0:T(4,128)} broadcast(f32[16,128,4]{2,1,0:T(8,128)S(1)} %copy-done.1), dimensions={0,1,2} | broadcast | bytes 8421376 | tf_op jit(solution)/shard_map/mul | solution.py:94
  155.0 10.7 %mul.180 = f32[16,128,1024]{2,1,0:T(8,128)} reshape(f32[16,128,4,256]{3,2,1,0:T(4,128)} %mul.155) | data formatting | bytes 16777216 | tf_op jit(solution)/shard_map/mul | solution.py:94
  165.8 0.0 all-to-all-done.1
  165.8 2.5 %fusion.20 = f32[8,1,8,256]{3,2,0,1:T(8,128)S(1)} fusion(bf16[8,8,4096]{2,1,0:T(8,128)(2,1)} %all-to-all-done.1, bf16[1,256,4096]{2,1,0:T(8,128)(2,1)} %param.32), kind=kOutput, calls=%fused_computation.23 | convolution fusion | flops 134217728 | bytes 2686976 | tf_op jit(solution)/shard_map/sxcd,xfd->sxcf/dot_general | solution.py:145
  168.3 2.5 %fusion.29 = bf16[8,1,8,256]{3,2,0,1:T(8,128)(2,1)S(1)} fusion(bf16[8,8,4096]{2,1,0:T(8,128)(2,1)} %all-to-all-done.1, bf16[1,256,4096]{2,1,0:T(8,128)(2,1)} %param.33, f32[8,1,8,256]{3,2,0,1:T(8,128)S(1)} %fusion.20), kind=kOutput, calls=%fused_computation.26 | convolution fusion | flops 134316032 | bytes 2719744 | tf_op jit(solution)/shard_map/sxcd,xfd->sxcf/dot_general | solution.py:148
  170.9 8.9 %all_gather.3 = bf16[8,1,8,1024]{3,2,0,1:T(8,128)(2,1)S(1)} all-gather(bf16[8,1,8,256]{3,2,0,1:T(8,128)(2,1)S(1)} %fusion.29), channel_id=1, replica_groups=mesh['ep'=8,'tp'=4] {'tp'}, dimensions={3}, use_global_device_ids=true | all-gather | bytes 163840 | tf_op jit(solution)/shard_map/all_gather | solution.py:154
  179.8 1.1 fusion.17
  180.9 5.1 %all-to-all-start.2 = ((bf16[8,8,1024]{2,1,0:T(8,128)(2,1)}), bf16[8,8,1024]{2,1,0:T(8,128)(2,1)S(1)}, u32[]{:S(2)}, u32[]{:S(2)}) async-start(bf16[8,8,1024]{2,1,0:T(8,128)(2,1)} %fusion.17), calls=%async_computation.3 | async-start | bytes 262144 | tf_op jit(solution)/shard_map/all_to_all | solution.py:161
  186.0 13.6 %multiply_add_fusion = f32[16,128,1024]{2,1,0:T(8,128)} fusion(f32[16,128,1024]{2,1,0:T(8,128)} %mul.180, f32[16,128,1024]{2,1,0:T(8,128)} %mul.178, f32[16,128,1024]{2,1,0:T(8,128)} %param.20, f32[16,1024]{1,0:T(8,128)S(1)} %get-tuple-element.4), kind=kLoop, calls=%fused_computation.2 | loop fusion | flops 6291456 | bytes 33619968 | tf_op jit(solution)/shard_map/add | solution.py:94
  199.6 0.0 all-to-all-done.2
  199.6 0.8 fusion.32
  (22 shorter events, 0.2 us)
Async XLA Ops:
  7.2 172.6 %copy-start = (bf16[1,1024,1024]{2,1,0:T(8,128)(2,1)S(1)}, bf16[1,1024,1024]{2,1,0:T(8,128)(2,1)}, u32[]{:S(2)}) copy-start(bf16[1,1024,1024]{2,1,0:T(8,128)(2,1)} %param.34) | copy-start | bytes 6291460
  10.1 13.1 %all-to-all-start = ((bf16[16,8,512]{2,0,1:T(8,128)(2,1)}), bf16[16,8,512]{2,0,1:T(8,128)(2,1)S(1)}, u32[]{:S(2)}, u32[]{:S(2)}) async-start(bf16[16,8,512]{2,0,1:T(8,128)(2,1)} %bitcast.84), calls=%async_computation | async-start | bytes 262144 | tf_op jit(solution)/shard_map/all_to_all | solution.py:55
  16.4 43.5 %reduce-scatter.2.cloned.1.call-start = ((), (), s32[]{:S(2)}) async-start(), calls=%async_computation.4 | async-start | bytes 1769472 | tf_op jit(solution)/shard_map/reduce_scatter | solution.py:57
  23.2 3.4 %copy-start.5 = (s32[16,2]{0,1:T(2,128)S(1)}, s32[16,2]{0,1:T(2,128)}, u32[]{:S(2)}) copy-start(s32[16,2]{0,1:T(2,128)} %param.35) | copy-start | bytes 388
  26.5 101.4 %all-reduce.2.cloned.1.call-start = ((), (), s32[]{:S(2)}) async-start(), calls=%async_computation.5 | async-start | bytes 262144 | tf_op jit(solution)/shard_map/psum | solution.py:116
  27.2 10.6 %copy-start.3 = (bf16[4096,64]{0,1:T(8,128)(2,1)S(1)}, bf16[4096,64]{0,1:T(8,128)(2,1)}, u32[]{:S(2)}) copy-start(bf16[4096,64]{0,1:T(8,128)(2,1)} %param.26) | copy-start | bytes 1572868
  69.6 14.1 %copy-start.6 = (f32[256]{0:T(256)S(1)}, f32[256]{0:T(256)}, u32[]{:S(2)}) copy-start(f32[256]{0:T(256)} %param.29) | copy-start | bytes 3076
  83.8 44.1 %copy-start.2 = (bf16[16,4096]{1,0:T(8,128)(2,1)S(1)}, bf16[16,4096]{1,0:T(8,128)(2,1)}, u32[]{:S(2)}) copy-start(bf16[16,4096]{1,0:T(8,128)(2,1)} %param.19) | copy-start | bytes 393220
  83.8 45.1 %copy-start.4 = (f32[4096]{0:T(1024)S(1)}, f32[4096]{0:T(1024)}, u32[]{:S(2)}) copy-start(f32[4096]{0:T(1024)} %param.31) | copy-start | bytes 49156
  83.8 50.9 %copy-start.7 = (f32[16,2]{0,1:T(2,128)S(1)}, f32[16,2]{0,1:T(2,128)}, u32[]{:S(2)}) copy-start(f32[16,2]{0,1:T(2,128)} %param.36) | copy-start | bytes 388
  83.8 50.9 %copy-start.8 = (f32[16]{0:T(128)S(1)}, f32[16]{0:T(128)}, u32[]{:S(2)}) copy-start(f32[16]{0:T(128)} %param.37) | copy-start | bytes 196
  130.1 35.7 %all-to-all-start.1 = ((bf16[8,8,4096]{2,1,0:T(8,128)(2,1)}), bf16[8,8,4096]{2,1,0:T(8,128)(2,1)}, u32[]{:S(2)}, u32[]{:S(2)}) async-start(bf16[8,8,4096]{2,1,0:T(8,128)(2,1)} %fusion.2), calls=%async_computation.2 | async-start | bytes 1048576 | tf_op jit(solution)/shard_map/all_to_all | solution.py:142
  139.4 11.1 %copy-start.1 = (f32[16,128,4]{2,1,0:T(8,128)S(1)}, f32[16,128,4]{2,1,0:T(8,128)}, u32[]{:S(2)}) copy-start(f32[16,128,4]{2,1,0:T(8,128)} %copy.41) | copy-start | bytes 98308
  180.9 18.7 %all-to-all-start.2 = ((bf16[8,8,1024]{2,1,0:T(8,128)(2,1)}), bf16[8,8,1024]{2,1,0:T(8,128)(2,1)S(1)}, u32[]{:S(2)}, u32[]{:S(2)}) async-start(bf16[8,8,1024]{2,1,0:T(8,128)(2,1)} %fusion.17), calls=%async_computation.3 | async-start | bytes 262144 | tf_op jit(solution)/shard_map/all_to_all | solution.py:161
Sparse Core Ops, SparseCore 0:
  26.6 33.2 reduce-scatter.1
  89.3 38.5 all-reduce.1
where the time goes:
time: 209 us; the launch traced here: 207 us
  waiting for transfers between devices  64.4 us (31%)
  local copies, waits for them, and re-layouts  45.8 us (22%)
  other arithmetic  25.8 us (12%)
  matrix products  21.6 us (10%)
  blocking collectives  19.2 us (9%)
  starting transfers between devices  16.1 us (8%)
  between operations  14.3 us (7%)
    psum x1, waiting for transfers between devices, on_device(): lax.psum(partial_out.astype(jnp.bfloat16), 'tp').astype(jnp.float32)  38.6 us
    mul x5, local copies, waits for them, and re-layouts, on_device(): updated = factor * state_four + key_part * value_part  30.7 us
    reduce_scatter x1, waiting for transfers between devices, on_device(): lax.psum_scatter(jnp.dot(spread, joined, preferred_element_type=jnp.float...  20.4 us
    add x2, other arithmetic, on_device(): updated = factor * state_four + key_part * value_part  20 us
    reshape x1, local copies, waits for them, and re-layouts, on_device(): previous_state.reshape(seq_count, KEY_CHANNELS, head_count, head_width)  10.6 us
    psum x1, blocking collectives, on_device(): totals = lax.psum(norm_table, 'tp')  10.2 us
    all_gather x1, blocking collectives, on_device(): lax.all_gather(hidden, 'tp', axis=3, tiled=True)  8.93 us
    all_to_all x1, starting transfers between devices, on_device(): lax.all_to_all(normed, 'ep', split_axis=1, concat_axis=0, tiled=True)  6.35 us
  transfers between devices with their start and end apart: 5, of which 3 were waited for; matrix products, arithmetic and copies ran while one was open for 28% of the time, Pallas kernels for 0%

commit v1 on v0

--- a/solution.py
+++ b/solution.py
@@ -1,12 +1,20 @@
+import functools
+
 import jax
 import jax.numpy as jnp
 from jax import lax
+from jax.experimental import pallas as pl
+from jax.experimental.pallas import tpu as pltpu
 from jax.sharding import PartitionSpec as P
 
 HEAD_TOTAL = 16
 KEY_CHANNELS = 128
 DV = 256
-
+GROUPS = 4
+STEP = 2
+F32 = jnp.float32
+BF16 = jnp.bfloat16
+MESH = pl.DeviceIdType.MESH
 
 epsilon = 1e-06
 forgetting_softness = 16.0
@@ -18,7 +26,7 @@
     return (scaled * gain_vec).astype(jnp.bfloat16)
 
 
-def on_device(
+def general(
     stream,
     previous_state,
     mixer_norm_gain,
@@ -169,6 +177,523 @@
     return (new_stream, updated.reshape(seq_count, KEY_CHANNELS, value_local))
 
 
+def greet(partners):
+    barrier = pltpu.get_barrier_semaphore()
+    for partner in partners:
+        pl.semaphore_signal(barrier, inc=1, device_id=partner, device_id_type=MESH)
+    pl.semaphore_wait(barrier, len(partners))
+
+
+def send(source, target, send_sem, recv_sem, partner):
+    copy = pltpu.make_async_remote_copy(
+        src_ref=source,
+        dst_ref=target,
+        send_sem=send_sem,
+        recv_sem=recv_sem,
+        device_id=partner,
+        device_id_type=MESH,
+    )
+    copy.start()
+    return copy
+
+
+def project_kernel(
+    n,
+    stream_ref,
+    gain_ref,
+    query_hbm,
+    key_hbm,
+    value_hbm,
+    gate_hbm,
+    lower_hbm,
+    upper_hbm,
+    boost_hbm,
+    fkq_ref,
+    value_ref,
+    gate_ref,
+    weights,
+    lower,
+    upper,
+    boost,
+    chunks,
+    spread,
+    pair_out,
+    pair_in,
+    own,
+    plane_out,
+    plane_in,
+    load_sem,
+    chunk_send,
+    chunk_recv,
+    pair_send,
+    pair_recv,
+    plane_send,
+    plane_recv,
+):
+    me = lax.axis_index("ep")
+    tp = lax.axis_index("tp")
+    core = lax.rem(me, 2)
+    row = me // 2
+    rows = n // 2
+    seqs = stream_ref.shape[0]
+    feats = chunks.shape[2]
+    span = boost.shape[1]
+    width = value_hbm.shape[1]
+    columns = pl.ds(pl.multiple_of(tp * span, 128), span)
+    loads = [
+        pltpu.make_async_copy(query_hbm.at[:, columns], weights.at[:, pl.ds(0, span)], load_sem.at[0]),
+        pltpu.make_async_copy(key_hbm.at[:, columns], weights.at[:, pl.ds(span, span)], load_sem.at[1]),
+        pltpu.make_async_copy(value_hbm, weights.at[:, pl.ds(2 * span, width)], load_sem.at[2]),
+        pltpu.make_async_copy(gate_hbm, weights.at[:, pl.ds(2 * span + width, width)], load_sem.at[3]),
+        pltpu.make_async_copy(lower_hbm, lower, load_sem.at[4]),
+        pltpu.make_async_copy(upper_hbm.at[:, columns], upper, load_sem.at[5]),
+        pltpu.make_async_copy(boost_hbm.at[:, columns], boost, load_sem.at[6]),
+    ]
+    for load in loads:
+        load.start()
+    floats = stream_ref[...].astype(F32)
+    scale = lax.rsqrt(jnp.mean(floats * floats, axis=-1, keepdims=True) + epsilon)
+    normed = (floats * scale * gain_ref[...]).astype(BF16)
+    for d in range(n):
+        chunks[d] = normed[:, d * feats : (d + 1) * feats]
+    greet([{"ep": lax.rem(me + d, n)} for d in range(1, n)])
+    sent = []
+    for d in range(1, n):
+        peer = lax.rem(me + d, n)
+        slot = row + rows * (d % 2)
+        sent.append(
+            send(chunks.at[peer], spread.at[slot], chunk_send.at[d], chunk_recv.at[d], {"ep": peer})
+        )
+    spread[row] = chunks[me]
+    for load in loads[4:]:
+        load.wait()
+    low_rank = jnp.dot(normed, lower[...], preferred_element_type=F32).astype(BF16)
+    logit = jnp.dot(low_rank, upper[...], preferred_element_type=F32)
+    log_sig = jnp.minimum(logit, 0.0) - jnp.log1p(jnp.exp(-jnp.abs(logit)))
+    factor = jnp.exp(log_sig / forgetting_softness - boost[...])
+    for load in loads[:4]:
+        load.wait()
+    for copy in sent:
+        copy.wait_recv()
+    half = rows * seqs
+    x = spread[...].reshape(n * seqs, feats)
+    cuts = [(0, 2 * span), (2 * span, width), (2 * span + width, width)]
+    partner = {"ep": me + 1 - 2 * core}
+    pairs = []
+    for b, (start, size) in enumerate(cuts):
+        part = jnp.dot(x, weights[:, start : start + size], preferred_element_type=F32)
+        pair_out[:, start : start + size] = part[half:].astype(BF16)
+        own[:, :, start : start + size] = part[:half].reshape(rows, seqs, size)
+        at = (slice(None), pl.ds(start, size))
+        pairs.append(
+            send(pair_out.at[at], pair_in.at[at], pair_send.at[b], pair_recv.at[b], partner)
+        )
+    planes = []
+    for b, (start, size) in enumerate(cuts):
+        pairs[b].wait_recv()
+        both = own[:, :, start : start + size] + pair_in[:, start : start + size].astype(
+            F32
+        ).reshape(rows, seqs, size)
+        own[:, :, start : start + size] = both
+        plane_out[:, :, start : start + size] = both.astype(BF16)
+        for d in range(1, rows):
+            there = lax.rem(row + d, rows)
+            planes.append(
+                send(
+                    plane_out.at[there, :, pl.ds(start, size)],
+                    plane_in.at[d, :, pl.ds(start, size)],
+                    plane_send.at[b, d],
+                    plane_recv.at[b, d],
+                    {"ep": there * 2 + core},
+                )
+            )
+    steps = seqs // STEP
+    for b, (start, size) in enumerate(cuts):
+        total = own[row, :, start : start + size]
+        for d in range(1, rows):
+            planes[b * (rows - 1) + d - 1].wait_recv()
+            total = total + plane_in[d, :, start : start + size].astype(F32)
+        if b == 0:
+            query = (total[:, :span] * KEY_CHANNELS ** (-0.5)).astype(BF16).astype(F32)
+            key = total[:, span:].astype(BF16).astype(F32)
+            for i in range(steps):
+                cut = slice(i * STEP, (i + 1) * STEP)
+                fkq_ref[i, 0:STEP] = factor[cut]
+                fkq_ref[i, STEP : 2 * STEP] = key[cut]
+                fkq_ref[i, 2 * STEP : 3 * STEP] = query[cut]
+                fkq_ref[i, 3 * STEP : 4 * STEP] = query[cut]
+        else:
+            target = value_ref if b == 1 else gate_ref
+            total = total.astype(BF16).astype(F32)
+            for i in range(steps):
+                target[i] = total[i * STEP : (i + 1) * STEP]
+    for copy in sent + pairs + planes:
+        copy.wait_send()
+
+
+def state_kernel(state_ref, fkq_ref, value_ref, gate_ref, gain_ref, out_ref, gated_ref):
+    heads = value_ref.shape[2] // DV
+    for h in range(heads):
+        turned = fkq_ref[0, :, h * KEY_CHANNELS : (h + 1) * KEY_CHANNELS].T
+        lanes = slice(h * DV, (h + 1) * DV)
+        for s in range(STEP):
+            factor = turned[:, s : s + 1]
+            key = turned[:, STEP + s : STEP + s + 1]
+            query = turned[:, 2 * STEP + s : 2 * STEP + s + 1]
+            updated = factor * state_ref[s, :, lanes] + key * value_ref[0, s : s + 1, lanes]
+            out_ref[s, :, lanes] = updated
+            readout = jnp.sum(query * updated, axis=0, keepdims=True)
+            mean_sq = jnp.mean(readout * readout, axis=-1, keepdims=True)
+            gate = gate_ref[0, s : s + 1, lanes]
+            silu = gate / (1.0 + jnp.exp(-gate))
+            gated_ref[0, s : s + 1, lanes] = (
+                readout * lax.rsqrt(mean_sq + epsilon) * gain_ref[...] * silu
+            )
+
+
+def mixture_kernel(
+    n,
+    m,
+    gated_ref,
+    stream_hbm,
+    gain_ref,
+    index_ref,
+    score_ref,
+    prob_ref,
+    output_hbm,
+    gate_hbm,
+    up_hbm,
+    down_hbm,
+    out_ref,
+    own_stream,
+    w_out,
+    w_gate,
+    w_up,
+    w_down,
+    lhs,
+    part_out,
+    part_in,
+    slots_out,
+    arrived,
+    hidden,
+    ready,
+    returned,
+    load_sem,
+    part_send,
+    part_recv,
+    slot_send,
+    slot_recv,
+    join_send,
+    join_recv,
+    hid_send,
+    hid_recv,
+    back_send,
+    back_recv,
+):
+    me = lax.axis_index("ep")
+    tp = lax.axis_index("tp")
+    seqs, width = own_stream.shape
+    capacity = arrived.shape[2]
+    others = [lax.rem(tp + d, m) for d in range(1, m)] + [tp]
+    loads = []
+    for j, there in enumerate(others):
+        cut = pl.ds(pl.multiple_of(there * width, 128), width)
+        loads.append(pltpu.make_async_copy(output_hbm.at[:, cut], w_out.at[j], load_sem.at[j]))
+    own_cut = pl.ds(pl.multiple_of(tp * width, 128), width)
+    loads += [
+        pltpu.make_async_copy(stream_hbm.at[:, own_cut], own_stream, load_sem.at[m]),
+        pltpu.make_async_copy(gate_hbm.at[0], w_gate, load_sem.at[m + 1]),
+        pltpu.make_async_copy(up_hbm.at[0], w_up, load_sem.at[m + 2]),
+        pltpu.make_async_copy(down_hbm.at[0], w_down, load_sem.at[m + 3]),
+    ]
+    for load in loads:
+        load.start()
+    for i in range(seqs // STEP):
+        lhs[i * STEP : (i + 1) * STEP] = gated_ref[i]
+    gated = lhs[...].astype(BF16)
+    greet(
+        [{"tp": there} for there in others[:-1]]
+        + [{"ep": lax.rem(me + d, n)} for d in range(1, n)]
+    )
+    parts = []
+    for j, there in enumerate(others):
+        loads[j].wait()
+        part = jnp.dot(gated, w_out[j], preferred_element_type=F32)
+        if j < m - 1:
+            part_out[j] = part.astype(BF16)
+            parts.append(
+                send(part_out.at[j], part_in.at[j], part_send.at[j], part_recv.at[j], {"tp": there})
+            )
+
+    index = index_ref[...]
+    group = index[:, 0:1] // (n // GROUPS)
+    lane = lax.broadcasted_iota(jnp.int32, (seqs, 128), 1)
+    one_hot = (lane == group).astype(F32)
+    earlier = lax.broadcasted_iota(jnp.int32, (seqs, seqs), 1) < lax.broadcasted_iota(
+        jnp.int32, (seqs, seqs), 0
+    )
+    counts = jnp.dot(earlier.astype(F32), one_hot, preferred_element_type=F32)
+    rank = jnp.sum(counts * one_hot, axis=1, keepdims=True).astype(jnp.int32)
+    slot_lane = lax.broadcasted_iota(jnp.int32, (seqs, GROUPS * capacity), 1)
+    placing = (slot_lane == group * capacity + rank).astype(F32)
+    scores = jnp.exp(score_ref[...])
+    weights = scores / jnp.sum(scores, axis=-1, keepdims=True) * prob_ref[...]
+    back_lane = lax.broadcasted_iota(jnp.int32, (seqs, n * capacity), 1)
+    combine = jnp.zeros((seqs, n * capacity), F32)
+    for k in range(index.shape[1]):
+        combine += jnp.where(
+            back_lane == index[:, k : k + 1] * capacity + rank, weights[:, k : k + 1], 0.0
+        )
+
+    loads[m].wait()
+    total = part
+    for j in range(m - 1):
+        parts[j].wait_recv()
+        total = total + part_in[j].astype(F32)
+    mixed = (own_stream[...].astype(F32) + total).astype(BF16)
+    slots = lax.dot_general(
+        placing, mixed.astype(F32), (((0,), (0,)), ((), ())), preferred_element_type=F32
+    )
+    slots_out[...] = slots.reshape(GROUPS, capacity, width).astype(BF16)
+    moved = []
+    per = n // GROUPS
+    for d in range(1, n):
+        peer = lax.rem(me + d, n)
+        moved.append(
+            send(
+                slots_out.at[peer // per],
+                arrived.at[tp, me],
+                slot_send.at[d],
+                slot_recv.at[d],
+                {"ep": peer},
+            )
+        )
+    arrived[tp, me] = slots_out[me // per]
+    for copy in moved:
+        copy.wait_recv()
+    joins = []
+    for j, there in enumerate(others[:-1]):
+        joins.append(
+            send(arrived.at[tp], arrived.at[tp], join_send.at[j], join_recv.at[j], {"tp": there})
+        )
+    for copy in joins:
+        copy.wait_recv()
+    square = jnp.zeros((n * capacity, 1), F32)
+    for t in range(m):
+        tokens = arrived[t].astype(F32).reshape(n * capacity, width)
+        square += jnp.sum(tokens * tokens, axis=-1, keepdims=True)
+    scale = lax.rsqrt(square / (m * width) + epsilon)
+    for load in loads[m + 1 : m + 3]:
+        load.wait()
+    nt = (((1,), (1,)), ((), ()))
+    gate_pre = jnp.zeros((n * capacity, w_gate.shape[0]), F32)
+    up_pre = jnp.zeros((n * capacity, w_gate.shape[0]), F32)
+    for t in range(m):
+        cut = slice(t * width, (t + 1) * width)
+        tokens = arrived[t].astype(F32).reshape(n * capacity, width)
+        normed = (tokens * scale * gain_ref[:, cut]).astype(BF16)
+        gate_pre += lax.dot_general(normed, w_gate[:, cut], nt, preferred_element_type=F32)
+        up_pre += lax.dot_general(normed, w_up[:, cut], nt, preferred_element_type=F32)
+    inner = gate_pre.shape[1]
+    hidden[tp] = (gate_pre / (1.0 + jnp.exp(-gate_pre)) * up_pre).astype(BF16)
+    shared = []
+    for j, there in enumerate(others[:-1]):
+        shared.append(
+            send(hidden.at[tp], hidden.at[tp], hid_send.at[j], hid_recv.at[j], {"tp": there})
+        )
+    loads[m + 3].wait()
+    for copy in shared:
+        copy.wait_recv()
+    outputs = jnp.zeros((n * capacity, width), F32)
+    for t in range(m):
+        outputs += jnp.dot(
+            hidden[t], w_down[t * inner : (t + 1) * inner, :], preferred_element_type=F32
+        )
+    ready[...] = outputs.reshape(n, capacity, width).astype(BF16)
+    backs = []
+    for d in range(1, n):
+        peer = lax.rem(me + d, n)
+        backs.append(
+            send(ready.at[peer], returned.at[me], back_send.at[d], back_recv.at[d], {"ep": peer})
+        )
+    returned[me] = ready[me]
+    for copy in backs:
+        copy.wait_recv()
+    rows = returned[...].astype(F32).reshape(n * capacity, width)
+    mixture = jnp.dot(
+        combine, rows, preferred_element_type=F32, precision=lax.Precision.HIGHEST
+    )
+    out_ref[...] = (mixed.astype(F32) + mixture).astype(BF16)
+    for copy in parts + moved + joins + shared + backs:
+        copy.wait_send()
+
+
+def fused(
+    stream,
+    previous_state,
+    mixer_norm_gain,
+    query_matrix,
+    key_matrix,
+    value_matrix,
+    output_gate_weight,
+    decay_lower_factor,
+    decay_upper_factor,
+    forgetting_boost,
+    head_norm_gain,
+    output_matrix,
+    mixture_norm_gain,
+    expert_gate_weight,
+    expert_up_weight,
+    expert_down_weight,
+    expert_index_table,
+    expert_scores_within,
+    group_probability,
+):
+    n = lax.axis_size("ep")
+    m = lax.axis_size("tp")
+    seqs, model = stream.shape
+    width = previous_state.shape[2]
+    span = width // DV * KEY_CHANNELS
+    feats = query_matrix.shape[0]
+    rank = decay_lower_factor.shape[1]
+    steps = seqs // STEP
+    total = 2 * span + 2 * width
+    rows = n // 2
+    half = rows * seqs
+    dma = pltpu.SemaphoreType.DMA
+    vmem = pl.BlockSpec(memory_space=pltpu.VMEM)
+    hbm = pl.BlockSpec(memory_space=pl.ANY)
+    fkq, values, gates = pl.pallas_call(
+        functools.partial(project_kernel, n),
+        name="project",
+        out_shape=(
+            jax.ShapeDtypeStruct((steps, 4 * STEP, span), F32),
+            jax.ShapeDtypeStruct((steps, STEP, width), F32),
+            jax.ShapeDtypeStruct((steps, STEP, width), F32),
+        ),
+        in_specs=[vmem, vmem] + [hbm] * 7,
+        out_specs=(vmem, vmem, vmem),
+        scratch_shapes=[
+            pltpu.VMEM((feats, total), BF16),
+            pltpu.VMEM((model, rank), BF16),
+            pltpu.VMEM((rank, span), BF16),
+            pltpu.VMEM((seqs, span), F32),
+            pltpu.VMEM((n, seqs, feats), BF16),
+            pltpu.VMEM((n, seqs, feats), BF16),
+            pltpu.VMEM((half, total), BF16),
+            pltpu.VMEM((half, total), BF16),
+            pltpu.VMEM((rows, seqs, total), F32),
+            pltpu.VMEM((rows, seqs, total), BF16),
+            pltpu.VMEM((rows, seqs, total), BF16),
+            dma((7,)),
+            dma((n,)),
+            dma((n,)),
+            dma((3,)),
+            dma((3,)),
+            dma((3, rows)),
+            dma((3, rows)),
+        ],
+        compiler_params=pltpu.CompilerParams(
+            collective_id=0, has_side_effects=True, vmem_limit_bytes=24 * 2**20
+        ),
+    )(
+        stream,
+        mixer_norm_gain.reshape(1, model),
+        query_matrix,
+        key_matrix,
+        value_matrix,
+        output_gate_weight,
+        decay_lower_factor,
+        decay_upper_factor,
+        forgetting_boost,
+    )
+    state_block = pl.BlockSpec((STEP, KEY_CHANNELS, width), lambda i: (i, 0, 0))
+    row_block = pl.BlockSpec((1, STEP, width), lambda i: (i, 0, 0))
+    new_state, gated = pl.pallas_call(
+        state_kernel,
+        name="state",
+        grid=(steps,),
+        out_shape=(
+            jax.ShapeDtypeStruct(previous_state.shape, F32),
+            jax.ShapeDtypeStruct((steps, STEP, width), F32),
+        ),
+        in_specs=[
+            state_block,
+            pl.BlockSpec((1, 4 * STEP, span), lambda i: (i, 0, 0)),
+            row_block,
+            row_block,
+            pl.BlockSpec((1, DV), lambda i: (0, 0)),
+        ],
+        out_specs=(state_block, row_block),
+        compiler_params=pltpu.CompilerParams(
+            dimension_semantics=("arbitrary",), vmem_limit_bytes=24 * 2**20
+        ),
+    )(previous_state, fkq, values, gates, head_norm_gain.reshape(1, DV))
+    inner = expert_gate_weight.shape[1]
+    deep = expert_down_weight.shape[1]
+    capacity = 2 * seqs * expert_index_table.shape[1] // n
+    new_stream = pl.pallas_call(
+        functools.partial(mixture_kernel, n, m),
+        name="mixture",
+        out_shape=jax.ShapeDtypeStruct((seqs, width), BF16),
+        in_specs=[vmem, hbm, vmem, vmem, vmem, vmem, hbm, hbm, hbm, hbm],
+        out_specs=vmem,
+        scratch_shapes=[
+            pltpu.VMEM((seqs, width), BF16),
+            pltpu.VMEM((m, width, width), BF16),
+            pltpu.VMEM((inner, model), BF16),
+            pltpu.VMEM((inner, model), BF16),
+            pltpu.VMEM((deep, width), BF16),
+            pltpu.VMEM((seqs, width), F32),
+            pltpu.VMEM((m - 1, seqs, width), BF16),
+            pltpu.VMEM((m - 1, seqs, width), BF16),
+            pltpu.VMEM((GROUPS, capacity, width), BF16),
+            pltpu.VMEM((m, n, capacity, width), BF16),
+            pltpu.VMEM((m, n * capacity, inner), BF16),
+            pltpu.VMEM((n, capacity, width), BF16),
+            pltpu.VMEM((n, capacity, width), BF16),
+            dma((m + 4,)),
+            dma((m - 1,)),
+            dma((m - 1,)),
+            dma((n,)),
+            dma((n,)),
+            dma((m - 1,)),
+            dma((m - 1,)),
+            dma((m - 1,)),
+            dma((m - 1,)),
+            dma((n,)),
+            dma((n,)),
+        ],
+        compiler_params=pltpu.CompilerParams(
+            collective_id=1, has_side_effects=True, vmem_limit_bytes=32 * 2**20
+        ),
+    )(
+        gated,
+        stream,
+        mixture_norm_gain.reshape(1, model),
+        expert_index_table,
+        expert_scores_within,
+        group_probability.reshape(seqs, 1),
+        output_matrix,
+        expert_gate_weight,
+        expert_up_weight,
+        expert_down_weight,
+    )
+    return (new_stream, new_state)
+
+
+def on_device(*arrays):
+    stream, state = arrays[0], arrays[1]
+    experts_held, route_count = arrays[13].shape[0], arrays[16].shape[1]
+    n = lax.axis_size("ep")
+    whole_heads = state.shape[2] % DV == 0
+    pair_routed = experts_held == 1 and n == GROUPS * route_count and route_count == 2
+    full_tiles = stream.shape[0] % 16 == 0 and stream.shape[1] == state.shape[2] * lax.axis_size("tp")
+    if whole_heads and pair_routed and full_tiles:
+        return fused(*arrays)
+    return general(*arrays)
+
+
 def solution(mesh):
     placed = (
         P("ep", None),

time: 209 us -> 86.7 us (0.41)
  Pallas kernels: 0 us -> 65.1 us
  waiting for transfers between devices: 64.4 us -> 0 us
  other arithmetic: 25.8 us -> 0 us
  local copies, waits for them, and re-layouts: 45.8 us -> 20.3 us
  matrix products: 21.6 us -> 0 us
  blocking collectives: 19.2 us -> 0 us
  starting transfers between devices: 16.1 us -> 0 us
  between operations: 14.3 us -> 0.74 us
    pallas_call x0 -> x3, Pallas kernels: none -> 65.1 us  [the longest x1 31.1 us: fused(): pl.pallas_call(functools.partial(mixture_kernel, n, m), name='mixture', o...]
    psum x1 -> x0, waiting for transfers between devices: 38.6 us -> none  [on_device(): lax.psum(partial_out.astype(jnp.bfloat16), 'tp').astype(jnp.float32)]
    mul x6 -> x0, local copies, waits for them, and re-layouts: 30.8 us -> none  [the longest x5 30.7 us: on_device(): updated = factor * state_four + key_part * value_part]
    dot_general x10 -> x0, matrix products: 21.6 us -> none  [the longest x1 5.31 us: on_device(): jnp.dot(gated_rows, output_matrix, preferred_element_type=jnp.float32)]
    reduce_scatter x1 -> x0, waiting for transfers between devices: 20.4 us -> none  [on_device(): lax.psum_scatter(jnp.dot(spread, joined, preferred_element_type=jnp.float...]
    unnamed x20 -> x42, local copies, waits for them, and re-layouts: 0.14 us -> 20.2 us
    add x3 -> x0, other arithmetic: 20 us -> none  [the longest x2 20 us: on_device(): updated = factor * state_four + key_part * value_part]
    all_to_all x3 -> x0, starting transfers between devices: 16.1 us -> none  [the longest x1 6.35 us: on_device(): lax.all_to_all(normed, 'ep', split_axis=1, concat_axis=0, tiled=True)]
  transfers between devices with their start and end apart: 5 -> 0, of which waited for: 3 -> 0; matrix products, arithmetic and copies ran while one was open for 28% -> 0% of each run, Pallas kernels for 0% -> 0%
where the time goes in v1:
time: 86.7 us; the launch traced here: 86.2 us
  Pallas kernels  65.1 us (75%)
  local copies, waits for them, and re-layouts  20.3 us (23%)
    pallas_call x1, Pallas kernels, fused(): pl.pallas_call(functools.partial(mixture_kernel, n, m), name='mixture', o...  31.1 us
    pallas_call x1, Pallas kernels, fused(): pl.pallas_call(functools.partial(project_kernel, n), name='project', out_...  22.3 us
    unnamed x42, local copies, waits for them, and re-layouts  20.2 us
    pallas_call x1, Pallas kernels, fused(): pl.pallas_call(state_kernel, name='state', grid=(steps,), out_shape=(jax....  11.7 us

profile of v1, /device:TPU:0, one launch (start us, length us, event | category | flops | bytes accessed | tf_op | source)
XLA Modules:
  0.0 86.2 jit_solution(2567620346970538409)
XLA Ops:
  0.6 0.0 copy-start.7
  0.6 1.6 %copy.21.lower_hbm = bf16[4096,64]{1,0:T(8,128)(2,1)S(1)} copy(bf16[4096,64]{0,1:T(8,128)(2,1)} %param.26) | data formatting | bytes 1048576 | tf_op args[7]
  2.2 0.0 copy-done.7
  2.3 0.0 copy-start.5
  2.3 1.6 %copy-done.5 = bf16[512,2048]{1,0:T(8,128)(2,1)S(1)} copy-done((bf16[512,2048]{1,0:T(8,128)(2,1)S(1)}, bf16[512,2048]{1,0:T(8,128)(2,1)}, u32[]{:S(2)}) %copy-start.5) | copy-done | bytes 2097176
  3.9 0.0 copy-start.6
  3.9 1.6 %copy-done.6 = bf16[512,2048]{1,0:T(8,128)(2,1)S(1)} copy-done((bf16[512,2048]{1,0:T(8,128)(2,1)S(1)}, bf16[512,2048]{1,0:T(8,128)(2,1)}, u32[]{:S(2)}) %copy-start.6) | copy-done | bytes 2097176
  5.4 0.0 copy-start.8
  5.4 1.2 %copy-done.8 = bf16[512,1024]{1,0:T(8,128)(2,1)S(1)} copy-done((bf16[512,1024]{1,0:T(8,128)(2,1)S(1)}, bf16[512,1024]{1,0:T(8,128)(2,1)}, u32[]{:S(2)}) %copy-start.8) | copy-done | bytes 1048600
  6.7 0.0 copy-start.9
  6.7 0.9 %copy-done.9 = bf16[16,4096]{1,0:T(8,128)(2,1)S(1)} copy-done((bf16[16,4096]{1,0:T(8,128)(2,1)S(1)}, bf16[16,4096]{1,0:T(8,128)(2,1)}, u32[]{:S(2)}) %copy-start.9) | copy-done | bytes 131096
  7.6 0.0 copy-start.11
  7.6 0.9 %copy-done.11 = bf16[64,2048]{1,0:T(8,128)(2,1)S(1)} copy-done((bf16[64,2048]{1,0:T(8,128)(2,1)S(1)}, bf16[64,2048]{1,0:T(8,128)(2,1)}, u32[]{:S(2)}) %copy-start.11) | copy-done | bytes 262168
  8.5 0.0 copy-start.12
  8.5 0.9 %copy-done.12 = f32[16,2048]{1,0:T(8,128)S(1)} copy-done((f32[16,2048]{1,0:T(8,128)S(1)}, f32[16,2048]{1,0:T(8,128)}, u32[]{:S(2)}) %copy-start.12) | copy-done | bytes 131096
  9.4 0.0 copy-start.13
  9.4 0.7 copy-done.13
  10.1 0.0 copy-start.15
  10.2 22.3 %project.1 = (f32[8,8,512]{2,1,0:T(8,128)S(1)}, f32[8,2,1024]{2,1,0:T(2,128)S(1)}, f32[8,2,1024]{2,1,0:T(2,128)S(1)}) custom-call(bf16[16,4096]{1,0:T(8,128)(2,1)S(1)} %copy-done.9, f32[1,4096]{1,0:T(1,128)S(1)} %bitcast.4, bf16[512,2048]{1,0:T(8,128)(2,1)S(1)} %copy-done.5, bf16[512,2048]{1,0:T(8,128)(2,1)S(1)} %copy-done.6, ...), custom_call_target="tpu_custom_call" | custom-call | tf_op jit(solution)/shard_map/project/pallas_call | solution.py:566
  32.5 0.0 copy-done.15
  32.5 0.0 copy-start
  32.5 3.4 %copy-done = f32[16,128,1024]{2,1,0:T(8,128)S(1)} copy-done((f32[16,128,1024]{2,1,0:T(8,128)S(1)}, f32[16,128,1024]{2,1,0:T(8,128)}, u32[]{:S(2)}) %copy-start) | copy-done | bytes 8388632
  35.9 0.0 copy-start.16
  35.9 0.0 copy-start.17
  35.9 0.0 copy-start.18
  35.9 0.0 copy-start.2
  35.9 0.0 copy-start.10
  35.9 0.0 copy-start.14
  35.9 11.7 %state.1 = (f32[16,128,1024]{2,1,0:T(8,128)}, f32[8,2,1024]{2,1,0:T(2,128)S(1)}) custom-call(f32[16,128,1024]{2,1,0:T(8,128)S(1)} %copy-done, f32[8,8,512]{2,1,0:T(8,128)S(1)} %get-tuple-element.7.fkq_ref, f32[8,2,1024]{2,1,0:T(2,128)S(1)} %get-tuple-element.8.value_ref, f32[8,2,1024]{2,1,0:T(2,128)S(1)} %get-tuple-element.9.gate_ref, f32[1,256]{1,0:T(1,128)S(1)} %bitcast.6), custom_call_target="tpu_custom_call" | custom-call | tf_op jit(solution)/shard_map/state/pallas_call | solution.py:612
  47.7 0.0 copy-done.16
  47.7 0.1 copy.22.index_ref
  47.8 0.0 copy-done.17
  47.8 0.1 copy.23.score_ref
  47.8 0.0 copy-done.18
  47.8 0.1 copy.24.prob_ref
  47.9 0.0 copy-done.2
  47.9 0.0 copy-done.10
  47.9 0.0 copy-done.14
  47.9 0.0 copy-start.1
  48.0 3.4 %copy-done.1 = bf16[1024,4096]{1,0:T(8,128)(2,1)S(1)} copy-done((bf16[1024,4096]{1,0:T(8,128)(2,1)S(1)}, bf16[1024,4096]{1,0:T(8,128)(2,1)}, u32[]{:S(2)}) %copy-start.1) | copy-done | bytes 8388632
  51.3 0.0 copy-start.3
  51.3 1.6 %copy-done.3 = bf16[1,256,4096]{2,1,0:T(8,128)(2,1)S(1)} copy-done((bf16[1,256,4096]{2,1,0:T(8,128)(2,1)S(1)}, bf16[1,256,4096]{2,1,0:T(8,128)(2,1)}, u32[]{:S(2)}) %copy-start.3) | copy-done | bytes 2097176
  52.9 0.0 copy-start.4
  52.9 1.6 %copy-done.4 = bf16[1,1024,1024]{2,1,0:T(8,128)(2,1)S(1)} copy-done((bf16[1,1024,1024]{2,1,0:T(8,128)(2,1)S(1)}, bf16[1,1024,1024]{2,1,0:T(8,128)(2,1)}, u32[]{:S(2)}) %copy-start.4) | copy-done | bytes 2097176
  54.5 31.1 %mixture.1 = bf16[16,1024]{1,0:T(8,128)(2,1)S(1)} custom-call(f32[8,2,1024]{2,1,0:T(2,128)S(1)} %get-tuple-element.10.gated_ref, bf16[16,4096]{1,0:T(8,128)(2,1)S(1)} %copy-done.10, f32[1,4096]{1,0:T(1,128)S(1)} %bitcast.5, s32[16,2]{1,0:T(8,128)S(1)} %copy.22.index_ref, f32[16,2]{1,0:T(8,128)S(1)} %copy.23.score_ref, f32[16,1]{1,0:T(8,128)S(1)} %copy.24.prob_ref, ...), custom_call_target="tpu_custom_call" | custom-call | tf_op jit(solution)/shard_map/mixture/pallas_call | solution.py:635
  85.6 0.6 copy.26
Async XLA Ops:
  0.6 1.6 %copy-start.7 = (bf16[512,1024]{1,0:T(8,128)(2,1)S(1)}, bf16[512,1024]{1,0:T(8,128)(2,1)}, u32[]{:S(2)}) copy-start(bf16[512,1024]{1,0:T(8,128)(2,1)} %value_hbm.1) | copy-start | bytes 3145732
  2.3 1.6 %copy-start.5 = (bf16[512,2048]{1,0:T(8,128)(2,1)S(1)}, bf16[512,2048]{1,0:T(8,128)(2,1)}, u32[]{:S(2)}) copy-start(bf16[512,2048]{1,0:T(8,128)(2,1)} %query_hbm.1) | copy-start | bytes 6291460
  3.9 1.6 %copy-start.6 = (bf16[512,2048]{1,0:T(8,128)(2,1)S(1)}, bf16[512,2048]{1,0:T(8,128)(2,1)}, u32[]{:S(2)}) copy-start(bf16[512,2048]{1,0:T(8,128)(2,1)} %key_hbm.1) | copy-start | bytes 6291460
  5.4 1.2 %copy-start.8 = (bf16[512,1024]{1,0:T(8,128)(2,1)S(1)}, bf16[512,1024]{1,0:T(8,128)(2,1)}, u32[]{:S(2)}) copy-start(bf16[512,1024]{1,0:T(8,128)(2,1)} %gate_hbm.2) | copy-start | bytes 3145732
  6.7 0.9 %copy-start.9 = (bf16[16,4096]{1,0:T(8,128)(2,1)S(1)}, bf16[16,4096]{1,0:T(8,128)(2,1)}, u32[]{:S(2)}) copy-start(bf16[16,4096]{1,0:T(8,128)(2,1)} %stream_hbm.1) | copy-start | bytes 393220
  7.6 0.9 %copy-start.11 = (bf16[64,2048]{1,0:T(8,128)(2,1)S(1)}, bf16[64,2048]{1,0:T(8,128)(2,1)}, u32[]{:S(2)}) copy-start(bf16[64,2048]{1,0:T(8,128)(2,1)} %upper_hbm.1) | copy-start | bytes 786436
  8.5 0.9 %copy-start.12 = (f32[16,2048]{1,0:T(8,128)S(1)}, f32[16,2048]{1,0:T(8,128)}, u32[]{:S(2)}) copy-start(f32[16,2048]{1,0:T(8,128)} %boost_hbm.1) | copy-start | bytes 393220
  9.4 0.7 copy-start.13
  10.1 22.3 %copy-start.15 = (f32[256]{0:T(256)S(1)}, f32[256]{0:T(256)}, u32[]{:S(2)}) copy-start(f32[256]{0:T(256)} %param.29) | copy-start | bytes 3076
  32.5 3.4 %copy-start = (f32[16,128,1024]{2,1,0:T(8,128)S(1)}, f32[16,128,1024]{2,1,0:T(8,128)}, u32[]{:S(2)}) copy-start(f32[16,128,1024]{2,1,0:T(8,128)} %state_ref.1) | copy-start | bytes 25165828
  35.9 11.8 %copy-start.16 = (s32[16,2]{0,1:T(2,128)S(1)}, s32[16,2]{0,1:T(2,128)}, u32[]{:S(2)}) copy-start(s32[16,2]{0,1:T(2,128)} %param.35) | copy-start | bytes 388
  35.9 11.9 %copy-start.17 = (f32[16,2]{0,1:T(2,128)S(1)}, f32[16,2]{0,1:T(2,128)}, u32[]{:S(2)}) copy-start(f32[16,2]{0,1:T(2,128)} %param.36) | copy-start | bytes 388
  35.9 12.0 %copy-start.18 = (f32[16]{0:T(128)S(1)}, f32[16]{0:T(128)}, u32[]{:S(2)}) copy-start(f32[16]{0:T(128)} %param.37) | copy-start | bytes 196
  35.9 12.0 %copy-start.2 = (bf16[1,256,4096]{2,1,0:T(8,128)(2,1)S(1)}, bf16[1,256,4096]{2,1,0:T(8,128)(2,1)}, u32[]{:S(2)}) copy-start(bf16[1,256,4096]{2,1,0:T(8,128)(2,1)} %gate_hbm.3) | copy-start | bytes 6291460
  35.9 12.0 %copy-start.10 = (bf16[16,4096]{1,0:T(8,128)(2,1)S(1)}, bf16[16,4096]{1,0:T(8,128)(2,1)}, u32[]{:S(2)}) copy-start(bf16[16,4096]{1,0:T(8,128)(2,1)} %stream_hbm.1) | copy-start | bytes 393220
  35.9 12.0 %copy-start.14 = (f32[4096]{0:T(1024)S(1)}, f32[4096]{0:T(1024)}, u32[]{:S(2)}) copy-start(f32[4096]{0:T(1024)} %param.31) | copy-start | bytes 49156
  47.9 3.4 %copy-start.1 = (bf16[1024,4096]{1,0:T(8,128)(2,1)S(1)}, bf16[1024,4096]{1,0:T(8,128)(2,1)}, u32[]{:S(2)}) copy-start(bf16[1024,4096]{1,0:T(8,128)(2,1)} %output_hbm.1) | copy-start | bytes 25165828
  51.3 1.6 %copy-start.3 = (bf16[1,256,4096]{2,1,0:T(8,128)(2,1)S(1)}, bf16[1,256,4096]{2,1,0:T(8,128)(2,1)}, u32[]{:S(2)}) copy-start(bf16[1,256,4096]{2,1,0:T(8,128)(2,1)} %up_hbm.1) | copy-start | bytes 6291460
  52.9 1.6 %copy-start.4 = (bf16[1,1024,1024]{2,1,0:T(8,128)(2,1)S(1)}, bf16[1,1024,1024]{2,1,0:T(8,128)(2,1)}, u32[]{:S(2)}) copy-start(bf16[1,1024,1024]{2,1,0:T(8,128)(2,1)} %down_hbm.1) | copy-start | bytes 6291460

commit v2 on v1

--- a/solution.py
+++ b/solution.py
@@ -12,6 +12,8 @@
 DV = 256
 GROUPS = 4
 STEP = 2
+COST = 20_000_000_000
+VM3 = 24
 F32 = jnp.float32
 BF16 = jnp.bfloat16
 MESH = pl.DeviceIdType.MESH
@@ -199,8 +201,8 @@
 
 def project_kernel(
     n,
-    stream_ref,
-    gain_ref,
+    stream_hbm,
+    gain_hbm,
     query_hbm,
     key_hbm,
     value_hbm,
@@ -211,6 +213,8 @@
     fkq_ref,
     value_ref,
     gate_ref,
+    stream,
+    gain,
     weights,
     lower,
     upper,
@@ -235,7 +239,7 @@
     core = lax.rem(me, 2)
     row = me // 2
     rows = n // 2
-    seqs = stream_ref.shape[0]
+    seqs = stream.shape[0]
     feats = chunks.shape[2]
     span = boost.shape[1]
     width = value_hbm.shape[1]
@@ -249,14 +253,20 @@
         pltpu.make_async_copy(upper_hbm.at[:, columns], upper, load_sem.at[5]),
         pltpu.make_async_copy(boost_hbm.at[:, columns], boost, load_sem.at[6]),
     ]
-    for load in loads:
+    first = [
+        pltpu.make_async_copy(stream_hbm, stream, load_sem.at[7]),
+        pltpu.make_async_copy(gain_hbm, gain, load_sem.at[8]),
+    ]
+    for load in first + loads:
         load.start()
-    floats = stream_ref[...].astype(F32)
+    greet([{"ep": lax.rem(me + d, n)} for d in range(1, n)])
+    for load in first:
+        load.wait()
+    floats = stream[...].astype(F32)
     scale = lax.rsqrt(jnp.mean(floats * floats, axis=-1, keepdims=True) + epsilon)
-    normed = (floats * scale * gain_ref[...]).astype(BF16)
+    normed = (floats * scale * gain[...]).astype(BF16)
     for d in range(n):
         chunks[d] = normed[:, d * feats : (d + 1) * feats]
-    greet([{"ep": lax.rem(me + d, n)} for d in range(1, n)])
     sent = []
     for d in range(1, n):
         peer = lax.rem(me + d, n)
@@ -267,7 +277,8 @@
     spread[row] = chunks[me]
     for load in loads[4:]:
         load.wait()
-    low_rank = jnp.dot(normed, lower[...], preferred_element_type=F32).astype(BF16)
+    nt = (((1,), (1,)), ((), ()))
+    low_rank = lax.dot_general(normed, lower[...], nt, preferred_element_type=F32).astype(BF16)
     logit = jnp.dot(low_rank, upper[...], preferred_element_type=F32)
     log_sig = jnp.minimum(logit, 0.0) - jnp.log1p(jnp.exp(-jnp.abs(logit)))
     factor = jnp.exp(log_sig / forgetting_softness - boost[...])
@@ -331,30 +342,51 @@
         copy.wait_send()
 
 
-def state_kernel(state_ref, fkq_ref, value_ref, gate_ref, gain_ref, out_ref, gated_ref):
-    heads = value_ref.shape[2] // DV
-    for h in range(heads):
-        turned = fkq_ref[0, :, h * KEY_CHANNELS : (h + 1) * KEY_CHANNELS].T
-        lanes = slice(h * DV, (h + 1) * DV)
+def state_kernel(state_ref, fkq_ref, value_ref, new_hbm, read_ref, turned, buffer, out_sem):
+    seqs, _, width = state_ref.shape
+    heads = width // DV
+    steps = seqs // STEP
+
+    def flush(i, slot):
+        return pltpu.make_async_copy(
+            buffer.at[slot], new_hbm.at[pl.ds(i * STEP, STEP)], out_sem.at[slot]
+        )
+
+    @pl.loop(0, steps)
+    def _(i):
+        slot = lax.rem(i, 2)
+
+        @pl.when(i >= 2)
+        def _():
+            flush(i - 2, slot).wait()
+
+        for h in range(heads):
+            turned[h] = fkq_ref[i, :, h * KEY_CHANNELS : (h + 1) * KEY_CHANNELS].T
         for s in range(STEP):
-            factor = turned[:, s : s + 1]
-            key = turned[:, STEP + s : STEP + s + 1]
-            query = turned[:, 2 * STEP + s : 2 * STEP + s + 1]
-            updated = factor * state_ref[s, :, lanes] + key * value_ref[0, s : s + 1, lanes]
-            out_ref[s, :, lanes] = updated
-            readout = jnp.sum(query * updated, axis=0, keepdims=True)
-            mean_sq = jnp.mean(readout * readout, axis=-1, keepdims=True)
-            gate = gate_ref[0, s : s + 1, lanes]
-            silu = gate / (1.0 + jnp.exp(-gate))
-            gated_ref[0, s : s + 1, lanes] = (
-                readout * lax.rsqrt(mean_sq + epsilon) * gain_ref[...] * silu
-            )
+            sums = []
+            for h in range(heads):
+                lanes = slice(h * DV, (h + 1) * DV)
+                factor = turned[h, :, s : s + 1]
+                key = turned[h, :, STEP + s : STEP + s + 1]
+                query = turned[h, :, 2 * STEP + s : 2 * STEP + s + 1]
+                updated = factor * state_ref[i * STEP + s, :, lanes] + key * value_ref[
+                    i, s : s + 1, lanes
+                ]
+                buffer[slot, s, :, lanes] = updated
+                sums.append(jnp.sum((query * updated).reshape(-1, 8, DV), axis=0))
+            read_ref[i * STEP + s] = jnp.concatenate(sums, axis=1)
+        flush(i, slot).start()
+
+    for i in range(steps - 2, steps):
+        flush(i, i % 2).wait()
 
 
 def mixture_kernel(
     n,
     m,
-    gated_ref,
+    read_ref,
+    rows_ref,
+    head_gain_ref,
     stream_hbm,
     gain_ref,
     index_ref,
@@ -385,6 +417,8 @@
     slot_recv,
     join_send,
     join_recv,
+    swap_send,
+    swap_recv,
     hid_send,
     hid_recv,
     back_send,
@@ -393,23 +427,32 @@
     me = lax.axis_index("ep")
     tp = lax.axis_index("tp")
     seqs, width = own_stream.shape
-    capacity = arrived.shape[2]
+    rows = n // 2
+    capacity = slots_out.shape[1]
     others = [lax.rem(tp + d, m) for d in range(1, m)] + [tp]
+    own_cut = pl.ds(pl.multiple_of(tp * width, 128), width)
+    load = pltpu.make_async_copy(stream_hbm.at[:, own_cut], own_stream, load_sem.at[m + 3])
     loads = []
     for j, there in enumerate(others):
         cut = pl.ds(pl.multiple_of(there * width, 128), width)
         loads.append(pltpu.make_async_copy(output_hbm.at[:, cut], w_out.at[j], load_sem.at[j]))
-    own_cut = pl.ds(pl.multiple_of(tp * width, 128), width)
     loads += [
-        pltpu.make_async_copy(stream_hbm.at[:, own_cut], own_stream, load_sem.at[m]),
-        pltpu.make_async_copy(gate_hbm.at[0], w_gate, load_sem.at[m + 1]),
-        pltpu.make_async_copy(up_hbm.at[0], w_up, load_sem.at[m + 2]),
-        pltpu.make_async_copy(down_hbm.at[0], w_down, load_sem.at[m + 3]),
+        pltpu.make_async_copy(gate_hbm, w_gate, load_sem.at[m]),
+        pltpu.make_async_copy(up_hbm, w_up, load_sem.at[m + 1]),
+        pltpu.make_async_copy(down_hbm, w_down, load_sem.at[m + 2]),
     ]
-    for load in loads:
-        load.start()
+    for one in loads + [load]:
+        one.start()
     for i in range(seqs // STEP):
-        lhs[i * STEP : (i + 1) * STEP] = gated_ref[i]
+        lhs[i * STEP : (i + 1) * STEP] = rows_ref[i]
+    gates = lhs[...]
+    silu = gates / (1.0 + jnp.exp(-gates))
+    readout = jnp.sum(read_ref[...], axis=1)
+    for h in range(width // DV):
+        lanes = slice(h * DV, (h + 1) * DV)
+        part = readout[:, lanes]
+        mean_sq = jnp.mean(part * part, axis=-1, keepdims=True)
+        lhs[:, lanes] = part * lax.rsqrt(mean_sq + epsilon) * head_gain_ref[...] * silu[:, lanes]
     gated = lhs[...].astype(BF16)
     greet(
         [{"tp": there} for there in others[:-1]]
@@ -445,7 +488,7 @@
             back_lane == index[:, k : k + 1] * capacity + rank, weights[:, k : k + 1], 0.0
         )
 
-    loads[m].wait()
+    load.wait()
     total = part
     for j in range(m - 1):
         parts[j].wait_recv()
@@ -455,45 +498,66 @@
         placing, mixed.astype(F32), (((0,), (0,)), ((), ())), preferred_element_type=F32
     )
     slots_out[...] = slots.reshape(GROUPS, capacity, width).astype(BF16)
+    core = lax.rem(me, 2)
+    row = me // 2
     moved = []
-    per = n // GROUPS
-    for d in range(1, n):
-        peer = lax.rem(me + d, n)
+    for d in range(1, rows):
+        there = lax.rem(row + d, rows)
         moved.append(
             send(
-                slots_out.at[peer // per],
-                arrived.at[tp, me],
+                slots_out.at[there],
+                arrived.at[tp, core, row],
                 slot_send.at[d],
                 slot_recv.at[d],
-                {"ep": peer},
+                {"ep": there * 2 + core},
             )
         )
-    arrived[tp, me] = slots_out[me // per]
+    arrived[tp, core, row] = slots_out[row]
     for copy in moved:
         copy.wait_recv()
     joins = []
     for j, there in enumerate(others[:-1]):
         joins.append(
-            send(arrived.at[tp], arrived.at[tp], join_send.at[j], join_recv.at[j], {"tp": there})
-        )
-    for copy in joins:
-        copy.wait_recv()
-    square = jnp.zeros((n * capacity, 1), F32)
-    for t in range(m):
-        tokens = arrived[t].astype(F32).reshape(n * capacity, width)
+            send(
+                arrived.at[tp, core],
+                arrived.at[tp, core],
+                join_send.at[j],
+                join_recv.at[j],
+                {"tp": there},
+            )
+        )
+    for one in loads[m:]:
+        one.wait()
+    swaps = []
+    nt = (((1,), (1,)), ((), ()))
+    tokens_held = n * capacity
+    square = jnp.zeros((tokens_held, 1), F32)
+    gate_pre = jnp.zeros((tokens_held, w_gate.shape[1]), F32)
+    up_pre = jnp.zeros((tokens_held, w_gate.shape[1]), F32)
+    origin = [tp] + [lax.rem(tp - 1 - j + m, m) for j in range(m - 1)]
+    for j, t in enumerate(origin):
+        if j > 0:
+            joins[j - 1].wait_recv()
+        swaps.append(
+            send(
+                arrived.at[t, core],
+                arrived.at[t, core],
+                swap_send.at[j],
+                swap_recv.at[j],
+                {"ep": me + 1 - 2 * core},
+            )
+        )
+    for j, t in enumerate(origin):
+        swaps[j].wait_recv()
+        cut = pl.ds(pl.multiple_of(t * width, 128), width)
+        tokens = arrived[t].astype(F32).reshape(tokens_held, width)
         square += jnp.sum(tokens * tokens, axis=-1, keepdims=True)
+        scaled = (tokens * gain_ref[:, cut]).astype(BF16)
+        gate_pre += lax.dot_general(scaled, w_gate[0, :, cut], nt, preferred_element_type=F32)
+        up_pre += lax.dot_general(scaled, w_up[0, :, cut], nt, preferred_element_type=F32)
     scale = lax.rsqrt(square / (m * width) + epsilon)
-    for load in loads[m + 1 : m + 3]:
-        load.wait()
-    nt = (((1,), (1,)), ((), ()))
-    gate_pre = jnp.zeros((n * capacity, w_gate.shape[0]), F32)
-    up_pre = jnp.zeros((n * capacity, w_gate.shape[0]), F32)
-    for t in range(m):
-        cut = slice(t * width, (t + 1) * width)
-        tokens = arrived[t].astype(F32).reshape(n * capacity, width)
-        normed = (tokens * scale * gain_ref[:, cut]).astype(BF16)
-        gate_pre += lax.dot_general(normed, w_gate[:, cut], nt, preferred_element_type=F32)
-        up_pre += lax.dot_general(normed, w_up[:, cut], nt, preferred_element_type=F32)
+    gate_pre *= scale
+    up_pre *= scale
     inner = gate_pre.shape[1]
     hidden[tp] = (gate_pre / (1.0 + jnp.exp(-gate_pre)) * up_pre).astype(BF16)
     shared = []
@@ -501,22 +565,27 @@
         shared.append(
             send(hidden.at[tp], hidden.at[tp], hid_send.at[j], hid_recv.at[j], {"tp": there})
         )
-    loads[m + 3].wait()
     for copy in shared:
         copy.wait_recv()
     outputs = jnp.zeros((n * capacity, width), F32)
     for t in range(m):
         outputs += jnp.dot(
-            hidden[t], w_down[t * inner : (t + 1) * inner, :], preferred_element_type=F32
+            hidden[t], w_down[0, t * inner : (t + 1) * inner, :], preferred_element_type=F32
         )
     ready[...] = outputs.reshape(n, capacity, width).astype(BF16)
     backs = []
     for d in range(1, n):
         peer = lax.rem(me + d, n)
         backs.append(
-            send(ready.at[peer], returned.at[me], back_send.at[d], back_recv.at[d], {"ep": peer})
-        )
-    returned[me] = ready[me]
+            send(
+                ready.at[lax.rem(peer, 2) * rows + peer // 2],
+                returned.at[me],
+                back_send.at[d],
+                back_recv.at[d],
+                {"ep": peer},
+            )
+        )
+    returned[me] = ready[core * rows + row]
     for copy in backs:
         copy.wait_recv()
     rows = returned[...].astype(F32).reshape(n * capacity, width)
@@ -524,7 +593,7 @@
         combine, rows, preferred_element_type=F32, precision=lax.Precision.HIGHEST
     )
     out_ref[...] = (mixed.astype(F32) + mixture).astype(BF16)
-    for copy in parts + moved + joins + shared + backs:
+    for copy in parts + moved + joins + swaps + shared + backs:
         copy.wait_send()
 
 
@@ -562,7 +631,7 @@
     half = rows * seqs
     dma = pltpu.SemaphoreType.DMA
     vmem = pl.BlockSpec(memory_space=pltpu.VMEM)
-    hbm = pl.BlockSpec(memory_space=pl.ANY)
+    hbm = pl.BlockSpec(memory_space=pltpu.HBM)
     fkq, values, gates = pl.pallas_call(
         functools.partial(project_kernel, n),
         name="project",
@@ -571,11 +640,13 @@
             jax.ShapeDtypeStruct((steps, STEP, width), F32),
             jax.ShapeDtypeStruct((steps, STEP, width), F32),
         ),
-        in_specs=[vmem, vmem] + [hbm] * 7,
-        out_specs=(vmem, vmem, vmem),
+        in_specs=[hbm] * 9,
+        out_specs=(vmem,) * 3,
         scratch_shapes=[
+            pltpu.VMEM((seqs, model), BF16),
+            pltpu.VMEM((1, model), F32),
             pltpu.VMEM((feats, total), BF16),
-            pltpu.VMEM((model, rank), BF16),
+            pltpu.VMEM((rank, model), BF16),
             pltpu.VMEM((rank, span), BF16),
             pltpu.VMEM((seqs, span), F32),
             pltpu.VMEM((n, seqs, feats), BF16),
@@ -585,7 +656,7 @@
             pltpu.VMEM((rows, seqs, total), F32),
             pltpu.VMEM((rows, seqs, total), BF16),
             pltpu.VMEM((rows, seqs, total), BF16),
-            dma((7,)),
+            dma((9,)),
             dma((n,)),
             dma((n,)),
             dma((3,)),
@@ -594,90 +665,94 @@
             dma((3, rows)),
         ],
         compiler_params=pltpu.CompilerParams(
-            collective_id=0, has_side_effects=True, vmem_limit_bytes=24 * 2**20
+            collective_id=0, has_side_effects=True, vmem_limit_bytes=12 * 2**20
         ),
+        cost_estimate=pl.CostEstimate(flops=COST, bytes_accessed=3 * feats * total, transcendentals=0),
     )(
-        stream,
-        mixer_norm_gain.reshape(1, model),
-        query_matrix,
-        key_matrix,
-        value_matrix,
-        output_gate_weight,
-        decay_lower_factor,
-        decay_upper_factor,
-        forgetting_boost,
-    )
-    state_block = pl.BlockSpec((STEP, KEY_CHANNELS, width), lambda i: (i, 0, 0))
-    row_block = pl.BlockSpec((1, STEP, width), lambda i: (i, 0, 0))
-    new_state, gated = pl.pallas_call(
+        *(pltpu.with_memory_space_constraint(a, pltpu.HBM) for a in (
+            stream,
+            mixer_norm_gain.reshape(1, model),
+            query_matrix,
+            key_matrix,
+            value_matrix,
+            output_gate_weight,
+            decay_lower_factor.T,
+            decay_upper_factor,
+            forgetting_boost,
+        ))
+    )
+    new_state, readout = pl.pallas_call(
         state_kernel,
         name="state",
-        grid=(steps,),
         out_shape=(
             jax.ShapeDtypeStruct(previous_state.shape, F32),
-            jax.ShapeDtypeStruct((steps, STEP, width), F32),
+            jax.ShapeDtypeStruct((seqs, 8, width), F32),
         ),
-        in_specs=[
-            state_block,
-            pl.BlockSpec((1, 4 * STEP, span), lambda i: (i, 0, 0)),
-            row_block,
-            row_block,
-            pl.BlockSpec((1, DV), lambda i: (0, 0)),
+        in_specs=[vmem, vmem, vmem],
+        out_specs=(hbm, vmem),
+        scratch_shapes=[
+            pltpu.VMEM((width // DV, KEY_CHANNELS, 4 * STEP), F32),
+            pltpu.VMEM((2, STEP, KEY_CHANNELS, width), F32),
+            dma((2,)),
         ],
-        out_specs=(state_block, row_block),
-        compiler_params=pltpu.CompilerParams(
-            dimension_semantics=("arbitrary",), vmem_limit_bytes=24 * 2**20
+        compiler_params=pltpu.CompilerParams(vmem_limit_bytes=6 * 2**20),
+        cost_estimate=pl.CostEstimate(
+            flops=COST // 4, bytes_accessed=4 * previous_state.size, transcendentals=0
         ),
-    )(previous_state, fkq, values, gates, head_norm_gain.reshape(1, DV))
+    )(previous_state, fkq, values)
     inner = expert_gate_weight.shape[1]
-    deep = expert_down_weight.shape[1]
     capacity = 2 * seqs * expert_index_table.shape[1] // n
     new_stream = pl.pallas_call(
         functools.partial(mixture_kernel, n, m),
         name="mixture",
         out_shape=jax.ShapeDtypeStruct((seqs, width), BF16),
-        in_specs=[vmem, hbm, vmem, vmem, vmem, vmem, hbm, hbm, hbm, hbm],
+        in_specs=[vmem] * 3 + [hbm] + [vmem] * 4 + [hbm] * 4,
         out_specs=vmem,
         scratch_shapes=[
             pltpu.VMEM((seqs, width), BF16),
             pltpu.VMEM((m, width, width), BF16),
-            pltpu.VMEM((inner, model), BF16),
-            pltpu.VMEM((inner, model), BF16),
-            pltpu.VMEM((deep, width), BF16),
+            pltpu.VMEM(expert_gate_weight.shape, BF16),
+            pltpu.VMEM(expert_up_weight.shape, BF16),
+            pltpu.VMEM(expert_down_weight.shape, BF16),
             pltpu.VMEM((seqs, width), F32),
             pltpu.VMEM((m - 1, seqs, width), BF16),
             pltpu.VMEM((m - 1, seqs, width), BF16),
             pltpu.VMEM((GROUPS, capacity, width), BF16),
-            pltpu.VMEM((m, n, capacity, width), BF16),
+            pltpu.VMEM((m, 2, rows, capacity, width), BF16),
             pltpu.VMEM((m, n * capacity, inner), BF16),
             pltpu.VMEM((n, capacity, width), BF16),
             pltpu.VMEM((n, capacity, width), BF16),
             dma((m + 4,)),
             dma((m - 1,)),
             dma((m - 1,)),
-            dma((n,)),
-            dma((n,)),
+            dma((rows,)),
+            dma((rows,)),
             dma((m - 1,)),
             dma((m - 1,)),
+            dma((m,)),
+            dma((m,)),
             dma((m - 1,)),
             dma((m - 1,)),
             dma((n,)),
             dma((n,)),
         ],
         compiler_params=pltpu.CompilerParams(
-            collective_id=1, has_side_effects=True, vmem_limit_bytes=32 * 2**20
+            collective_id=1, has_side_effects=True, vmem_limit_bytes=VM3 * 2**20
         ),
+        cost_estimate=pl.CostEstimate(flops=COST, bytes_accessed=2 * output_matrix.size, transcendentals=0),
     )(
-        gated,
+        readout,
+        gates,
+        head_norm_gain.reshape(1, DV),
         stream,
         mixture_norm_gain.reshape(1, model),
         expert_index_table,
         expert_scores_within,
         group_probability.reshape(seqs, 1),
-        output_matrix,
-        expert_gate_weight,
-        expert_up_weight,
-        expert_down_weight,
+        *(
+            pltpu.with_memory_space_constraint(a, pltpu.HBM)
+            for a in (output_matrix, expert_gate_weight, expert_up_weight, expert_down_weight)
+        ),
     )
     return (new_stream, new_state)
 

time: 86.7 us -> 57.4 us (0.66)
  local copies, waits for them, and re-layouts: 20.3 us -> 0.91 us
  Pallas kernels: 65.1 us -> 55.6 us
    unnamed x42 -> x17, local copies, waits for them, and re-layouts: 20.2 us -> 0.83 us
    pallas_call x1, Pallas kernels: 31.1 us -> 26.5 us  [fused(): pl.pallas_call(functools.partial(mixture_kernel, n, m), name='mixture', o...]
    pallas_call x1, Pallas kernels: 11.7 us -> 7.16 us  [fused(): pl.pallas_call(state_kernel, name='state', out_shape=(jax.ShapeDtypeStruc...]
where the time goes in v2:
time: 57.4 us; the launch traced here: 57.2 us
  Pallas kernels  55.6 us (97%)
  local copies, waits for them, and re-layouts  0.91 us (2%)
  between operations  0.74 us (1%)
    pallas_call x1, Pallas kernels, fused(): pl.pallas_call(functools.partial(mixture_kernel, n, m), name='mixture', o...  26.5 us
    pallas_call x1, Pallas kernels, fused(): pl.pallas_call(functools.partial(project_kernel, n), name='project', out_...  22 us
    pallas_call x1, Pallas kernels, fused(): pl.pallas_call(state_kernel, name='state', out_shape=(jax.ShapeDtypeStruc...  7.16 us

profile of v2, /device:TPU:0, one launch (start us, length us, event | category | flops | bytes accessed | tf_op | source)
XLA Modules:
  0.0 57.2 jit_solution(14922990652433488527)
XLA Ops:
  0.6 0.0 copy-start
  0.6 22.0 %project.1 = (f32[8,8,512]{2,1,0:T(8,128)S(1)}, f32[8,2,1024]{2,1,0:T(2,128)S(1)}, f32[8,2,1024]{2,1,0:T(2,128)S(1)}) custom-call(bf16[16,4096]{1,0:T(8,128)(2,1)} %stream_hbm.3, f32[1,4096]{1,0:T(1,128)} %bitcast.9, bf16[512,2048]{1,0:T(8,128)(2,1)} %query_hbm.1, bf16[512,2048]{1,0:T(8,128)(2,1)} %key_hbm.1, bf16[512,1024]{1,0:T(8,128)(2,1)} %value_hbm.1, ...), custom_call_target="tpu_custom_call" | custom-call | flops 20000000000 | bytes 4718592 | tf_op jit(solution)/shard_map/project/pallas_call | solution.py:635
  22.6 0.0 copy-done
  22.6 0.0 copy-start.4
  22.7 0.0 copy-start.5
  22.7 0.0 copy-start.6
  22.7 0.0 copy-start.1
  22.7 0.0 copy-start.2
  22.7 0.0 copy-start.3
  22.7 7.2 %state.1 = (f32[16,128,1024]{2,1,0:T(8,128)}, f32[16,8,1024]{2,1,0:T(8,128)S(1)}) custom-call(f32[16,128,1024]{2,1,0:T(8,128)S(1)} %copy-done, f32[8,8,512]{2,1,0:T(8,128)S(1)} %get-tuple-element.7.fkq_ref, f32[8,2,1024]{2,1,0:T(2,128)S(1)} %get-tuple-element.8.value_ref), custom_call_target="tpu_custom_call" | custom-call | flops 5000000000 | bytes 8388608 | tf_op jit(solution)/shard_map/state/pallas_call | solution.py:684
  29.9 0.0 copy-done.4
  29.9 0.1 copy.21.index_ref
  30.0 0.0 copy-done.5
  30.0 0.1 copy.22.score_ref
  30.1 0.0 copy-done.6
  30.1 0.1 copy.23.prob_ref
  30.2 0.0 copy-done.1
  30.2 0.0 copy-done.2
  30.2 0.0 copy-done.3
  30.2 26.5 %mixture.1 = bf16[16,1024]{1,0:T(8,128)(2,1)S(1)} custom-call(f32[16,8,1024]{2,1,0:T(8,128)S(1)} %get-tuple-element.9.read_ref, f32[8,2,1024]{2,1,0:T(2,128)S(1)} %get-tuple-element.10.rows_ref, f32[1,256]{1,0:T(1,128)S(1)} %bitcast.6, bf16[16,4096]{1,0:T(8,128)(2,1)S(1)} %copy-done.1, f32[1,4096]{1,0:T(1,128)S(1)} %bitcast.5, s32[16,2]{1,0:T(8,128)S(1)} %copy.21.index_ref, ...), custom_call_target="tpu_custom_call" | custom-call | flops 20000000000 | bytes 8388608 | tf_op jit(solution)/shard_map/mixture/pallas_call | solution.py:705
  56.6 0.6 %copy.25 = bf16[16,1024]{1,0:T(8,128)(2,1)} copy(bf16[16,1024]{1,0:T(8,128)(2,1)S(1)} %mixture.1) | data formatting | bytes 65536
Async XLA Ops:
  0.6 22.0 %copy-start = (f32[16,128,1024]{2,1,0:T(8,128)S(1)}, f32[16,128,1024]{2,1,0:T(8,128)}, u32[]{:S(2)}) copy-start(f32[16,128,1024]{2,1,0:T(8,128)} %state_ref.1) | copy-start | bytes 25165828
  22.6 7.2 %copy-start.4 = (s32[16,2]{0,1:T(2,128)S(1)}, s32[16,2]{0,1:T(2,128)}, u32[]{:S(2)}) copy-start(s32[16,2]{0,1:T(2,128)} %param.35) | copy-start | bytes 388
  22.7 7.3 %copy-start.5 = (f32[16,2]{0,1:T(2,128)S(1)}, f32[16,2]{0,1:T(2,128)}, u32[]{:S(2)}) copy-start(f32[16,2]{0,1:T(2,128)} %param.36) | copy-start | bytes 388
  22.7 7.4 %copy-start.6 = (f32[16]{0:T(128)S(1)}, f32[16]{0:T(128)}, u32[]{:S(2)}) copy-start(f32[16]{0:T(128)} %param.37) | copy-start | bytes 196
  22.7 7.5 %copy-start.1 = (bf16[16,4096]{1,0:T(8,128)(2,1)S(1)}, bf16[16,4096]{1,0:T(8,128)(2,1)}, u32[]{:S(2)}) copy-start(bf16[16,4096]{1,0:T(8,128)(2,1)} %stream_hbm.3) | copy-start | bytes 393220
  22.7 7.5 %copy-start.2 = (f32[4096]{0:T(1024)S(1)}, f32[4096]{0:T(1024)}, u32[]{:S(2)}) copy-start(f32[4096]{0:T(1024)} %param.31) | copy-start | bytes 49156
  22.7 7.4 %copy-start.3 = (f32[256]{0:T(256)S(1)}, f32[256]{0:T(256)}, u32[]{:S(2)}) copy-start(f32[256]{0:T(256)} %param.29) | copy-start | bytes 3076

commit v3 on v2

--- a/solution.py
+++ b/solution.py
@@ -11,7 +11,7 @@
 KEY_CHANNELS = 128
 DV = 256
 GROUPS = 4
-STEP = 2
+STEP = 4
 COST = 20_000_000_000
 VM3 = 24
 F32 = jnp.float32
@@ -695,7 +695,7 @@
             pltpu.VMEM((2, STEP, KEY_CHANNELS, width), F32),
             dma((2,)),
         ],
-        compiler_params=pltpu.CompilerParams(vmem_limit_bytes=6 * 2**20),
+        compiler_params=pltpu.CompilerParams(vmem_limit_bytes=10 * 2**20),
         cost_estimate=pl.CostEstimate(
             flops=COST // 4, bytes_accessed=4 * previous_state.size, transcendentals=0
         ),

time: 57.4 us -> 56.2 us (0.979)
  Pallas kernels: 55.6 us -> 54.4 us
    pallas_call x1, Pallas kernels: 7.16 us -> 5.94 us  [fused(): pl.pallas_call(state_kernel, name='state', out_shape=(jax.ShapeDtypeStruc...]
where the time goes in v3:
time: 56.2 us; the launch traced here: 56 us
  Pallas kernels  54.4 us (97%)
  local copies, waits for them, and re-layouts  0.91 us (2%)
  between operations  0.74 us (1%)
    pallas_call x1, Pallas kernels, fused(): pl.pallas_call(functools.partial(mixture_kernel, n, m), name='mixture', o...  26.4 us
    pallas_call x1, Pallas kernels, fused(): pl.pallas_call(functools.partial(project_kernel, n), name='project', out_...  22 us
    pallas_call x1, Pallas kernels, fused(): pl.pallas_call(state_kernel, name='state', out_shape=(jax.ShapeDtypeStruc...  5.94 us

profile of v3, /device:TPU:0, one launch (start us, length us, event | category | flops | bytes accessed | tf_op | source)
XLA Modules:
  0.0 56.0 jit_solution(10152801564626851734)
XLA Ops:
  0.6 0.0 copy-start
  0.6 22.0 %project.1 = (f32[4,16,512]{2,1,0:T(8,128)S(1)}, f32[4,4,1024]{2,1,0:T(4,128)S(1)}, f32[4,4,1024]{2,1,0:T(4,128)S(1)}) custom-call(bf16[16,4096]{1,0:T(8,128)(2,1)} %stream_hbm.3, f32[1,4096]{1,0:T(1,128)} %bitcast.9, bf16[512,2048]{1,0:T(8,128)(2,1)} %query_hbm.1, bf16[512,2048]{1,0:T(8,128)(2,1)} %key_hbm.1, bf16[512,1024]{1,0:T(8,128)(2,1)} %value_hbm.1, ...), custom_call_target="tpu_custom_call" | custom-call | flops 20000000000 | bytes 4718592 | tf_op jit(solution)/shard_map/project/pallas_call | solution.py:635
  22.6 0.0 copy-done
  22.6 0.0 copy-start.4
  22.7 0.0 copy-start.5
  22.7 0.0 copy-start.6
  22.7 0.0 copy-start.1
  22.7 0.0 copy-start.2
  22.7 0.0 copy-start.3
  22.7 5.9 %state.1 = (f32[16,128,1024]{2,1,0:T(8,128)}, f32[16,8,1024]{2,1,0:T(8,128)S(1)}) custom-call(f32[16,128,1024]{2,1,0:T(8,128)S(1)} %copy-done, f32[4,16,512]{2,1,0:T(8,128)S(1)} %get-tuple-element.7.fkq_ref, f32[4,4,1024]{2,1,0:T(4,128)S(1)} %get-tuple-element.8.value_ref), custom_call_target="tpu_custom_call" | custom-call | flops 5000000000 | bytes 8388608 | tf_op jit(solution)/shard_map/state/pallas_call | solution.py:684
  28.7 0.0 copy-done.4
  28.7 0.1 copy.21.index_ref
  28.8 0.0 copy-done.5
  28.8 0.1 copy.22.score_ref
  28.8 0.0 copy-done.6
  28.8 0.1 copy.23.prob_ref
  28.9 0.0 copy-done.1
  28.9 0.0 copy-done.2
  28.9 0.0 copy-done.3
  28.9 26.4 %mixture.1 = bf16[16,1024]{1,0:T(8,128)(2,1)S(1)} custom-call(f32[16,8,1024]{2,1,0:T(8,128)S(1)} %get-tuple-element.9.read_ref, f32[4,4,1024]{2,1,0:T(4,128)S(1)} %get-tuple-element.10.rows_ref, f32[1,256]{1,0:T(1,128)S(1)} %bitcast.6, bf16[16,4096]{1,0:T(8,128)(2,1)S(1)} %copy-done.1, f32[1,4096]{1,0:T(1,128)S(1)} %bitcast.5, s32[16,2]{1,0:T(8,128)S(1)} %copy.21.index_ref, ...), custom_call_target="tpu_custom_call" | custom-call | flops 20000000000 | bytes 8388608 | tf_op jit(solution)/shard_map/mixture/pallas_call | solution.py:705
  55.4 0.6 %copy.25 = bf16[16,1024]{1,0:T(8,128)(2,1)} copy(bf16[16,1024]{1,0:T(8,128)(2,1)S(1)} %mixture.1) | data formatting | bytes 65536
Async XLA Ops:
  0.6 22.0 %copy-start = (f32[16,128,1024]{2,1,0:T(8,128)S(1)}, f32[16,128,1024]{2,1,0:T(8,128)}, u32[]{:S(2)}) copy-start(f32[16,128,1024]{2,1,0:T(8,128)} %state_ref.1) | copy-start | bytes 25165828
  22.6 6.0 %copy-start.4 = (s32[16,2]{0,1:T(2,128)S(1)}, s32[16,2]{0,1:T(2,128)}, u32[]{:S(2)}) copy-start(s32[16,2]{0,1:T(2,128)} %param.35) | copy-start | bytes 388
  22.7 6.1 %copy-start.5 = (f32[16,2]{0,1:T(2,128)S(1)}, f32[16,2]{0,1:T(2,128)}, u32[]{:S(2)}) copy-start(f32[16,2]{0,1:T(2,128)} %param.36) | copy-start | bytes 388
  22.7 6.2 %copy-start.6 = (f32[16]{0:T(128)S(1)}, f32[16]{0:T(128)}, u32[]{:S(2)}) copy-start(f32[16]{0:T(128)} %param.37) | copy-start | bytes 196
  22.7 6.3 %copy-start.1 = (bf16[16,4096]{1,0:T(8,128)(2,1)S(1)}, bf16[16,4096]{1,0:T(8,128)(2,1)}, u32[]{:S(2)}) copy-start(bf16[16,4096]{1,0:T(8,128)(2,1)} %stream_hbm.3) | copy-start | bytes 393220
  22.7 6.2 %copy-start.2 = (f32[4096]{0:T(1024)S(1)}, f32[4096]{0:T(1024)}, u32[]{:S(2)}) copy-start(f32[4096]{0:T(1024)} %param.31) | copy-start | bytes 49156
  22.7 6.2 %copy-start.3 = (f32[256]{0:T(256)S(1)}, f32[256]{0:T(256)}, u32[]{:S(2)}) copy-start(f32[256]{0:T(256)} %param.29) | copy-start | bytes 3076
